TPU v7x, 512 devices: a 4x2x32 block of a 4x8x32 slice. The times are simulated.
512 devices in a mesh: grp: 2 (over y), fs: 32 (over z), tp: 8 (over x, core).
Axes of the slice: x: 4, y: 2, z: 32, core: 2. Of those that a mesh axis runs over, the one named last changes fastest.
The devices are a block of a 4x8x32 slice.
Arguments:
- tokens: bfloat16 [12288, 2048], P(('grp', 'fs'), 'tp'), parts along dimension 0, may hold values from -40 to 40
- routes: int32 [12288, 8], P(('grp', 'fs')), parts along dimension 0, may hold values from 0 to 31, all different within a row; in each aligned block of 192 rows (0 to 191, 192 to 383, ...) at most 56 rows name the same one
- routing_weight: float32 [12288, 8], P(('grp', 'fs')), parts along dimension 0, may hold values from 0.1 to 0.6
- norm_gain_vector: float32 [2048], P('tp'), may hold values from 0.1 to 1.9
- expert_gate: float32 [32, 512, 2048], P(None, 'fs', 'tp'), may hold values from -0.125 to 0.125
- expert_up: float32 [32, 512, 2048], P(None, 'fs', 'tp'), may hold values from -0.125 to 0.125
- expert_down: float32 [32, 512, 2048], P(None, 'fs', 'tp'), may hold values from -0.25 to 0.25
- shared_gate: float32 [512, 2048], P('fs', 'tp'), may hold values from -0.125 to 0.125
- shared_up: float32 [512, 2048], P('fs', 'tp'), may hold values from -0.125 to 0.125
- shared_down: float32 [512, 2048], P('fs', 'tp'), may hold values from -0.25 to 0.25
Outputs:
- mixed: bfloat16 [12288, 2048], P(('grp', 'fs'), 'tp'), parts along dimension 0
- gate_served: bfloat16 [64, 512, 2048], P(('grp', 'fs'), None, 'tp'), parts along dimension 0
- up_served: bfloat16 [64, 512, 2048], P(('grp', 'fs'), None, 'tp'), parts along dimension 0
- down_served: bfloat16 [64, 512, 2048], P(('grp', 'fs'), None, 'tp'), parts along dimension 0
- shared_gate_served: bfloat16 [1024, 2048], P('grp', 'tp'), parts along dimension 0
- shared_up_served: bfloat16 [1024, 2048], P('grp', 'tp'), parts along dimension 0
- shared_down_served: bfloat16 [1024, 2048], P('grp', 'tp'), parts along dimension 0
There are 2 independent parts, one for each index of `grp`. A program takes and returns all parts, laid end to end along the dimension named above; an argument that names none is the same for every part. Nothing has to cross between parts.
Inputs may be any that keep to these rules, and one draw needn't show every extreme that they name: `routes`: each row names 8 different experts. In each aligned block of 192 rows no expert is named by more than 56 rows, and in some block an expert is named by exactly 56 rows.
All inputs are finite; a program needn't handle non-finite values.
Results may differ from a plain program's by a relative error of at most 0.022.
Values may be sent and summed in bfloat16 or wider, within the bound.
No kernel may reach another device: no remote copies, remote signals or barrier semaphores. Data moves between devices by JAX's collectives and lax.ppermute only.
A program may use at most 64 MiB of HBM per device.

v0:
```python
import jax
import jax.numpy as jnp
from jax import lax
from jax.sharding import PartitionSpec as P

norm_eps = 1e-06


def sent_together(arrays, axis, split_dim, concat_dim, along):
    widths = [a.shape[along] for a in arrays]
    both = jnp.concatenate(arrays, axis=along)
    out = lax.all_to_all(both, axis, split_axis=split_dim, concat_axis=concat_dim, tiled=True)
    return tuple(jnp.split(out, [sum(widths[:k]) for k in range(1, len(widths))], axis=along))


def sent_together_2(arrays, axis, dim, along):
    both = jnp.concatenate(arrays, axis=along)
    out, at, outs = (lax.all_gather(both, axis, axis=dim, tiled=True), 0, [])
    for a in arrays:
        outs.append(lax.slice_in_dim(out, at, at + a.shape[along], axis=along))
        at += a.shape[along]
    return tuple(outs)


def in_one_piece(arrays, axis, dim, along):
    both = jnp.concatenate(arrays, axis=along)
    out, at, outs = (lax.psum_scatter(both, axis, scatter_dimension=dim, tiled=True), 0, [])
    for a in arrays:
        outs.append(lax.slice_in_dim(out, at, at + a.shape[along], axis=along))
        at += a.shape[along]
    return tuple(outs)


def dense_rows(rows, weight):
    return lax.dot_general(
        rows, weight, (((1,), (1,)), ((), ())), preferred_element_type=jnp.float32
    )


def per_device(
    tokens,
    routes,
    routing_weight,
    norm_gain_vector,
    expert_gate,
    expert_up,
    expert_down,
    shared_gate,
    shared_up,
    shared_down,
):
    tok_rows, portion_width = tokens.shape
    model_width = portion_width * lax.axis_size("tp")
    experts = expert_gate.shape[0]
    top_count = routes.shape[1]
    capacity = tok_rows * top_count * 7 // (6 * experts)
    gate_round = (expert_gate * norm_gain_vector[None, None, :]).astype(jnp.bfloat16)
    up_round = (expert_up * norm_gain_vector[None, None, :]).astype(jnp.bfloat16)
    down_round = expert_down.astype(jnp.bfloat16)
    gate_refreshed, up_new, down_new = sent_together(
        (gate_round, up_round, down_round), "fs", 0, 1, 2
    )
    shared_g, shared_u, shared_d = sent_together_2(
        (
            (shared_gate * norm_gain_vector[None, :]).astype(jnp.bfloat16),
            (shared_up * norm_gain_vector[None, :]).astype(jnp.bfloat16),
            shared_down.astype(jnp.bfloat16),
        ),
        "fs",
        0,
        1,
    )
    values = tokens.astype(jnp.float32)
    totals = lax.psum(jnp.sum(values * values, axis=1), "tp")
    normed = (values * lax.rsqrt(totals / model_width + norm_eps)[:, None]).astype(jnp.bfloat16)
    flat_expert = routes.reshape(-1)
    onehot = (flat_expert[:, None] == jnp.arange(experts, dtype=jnp.int32)[None, :]).astype(
        jnp.int32
    )
    earlier = jnp.cumsum(onehot, axis=0) - onehot
    slot_index = jnp.sum(earlier * onehot, axis=1)
    target = (flat_expert * capacity + slot_index).reshape(tok_rows, top_count)
    places = jnp.arange(experts * capacity, dtype=jnp.int32)
    placing = jnp.sum(
        (target[:, :, None] == places[None, None, :]).astype(jnp.int32), axis=1
    ).astype(jnp.bfloat16)
    outgoing = lax.dot_general(
        placing, normed, (((0,), (0,)), ((), ())), preferred_element_type=jnp.float32
    ).astype(jnp.bfloat16)
    incoming = lax.all_to_all(
        outgoing.reshape(experts, capacity, portion_width),
        "fs",
        split_axis=0,
        concat_axis=0,
        tiled=True,
    )
    arrived = incoming.reshape(experts * capacity, portion_width)
    partials = (
        dense_rows(arrived, gate_refreshed[0]).astype(jnp.bfloat16),
        dense_rows(arrived, up_new[0]).astype(jnp.bfloat16),
        dense_rows(normed, shared_g).astype(jnp.bfloat16),
        dense_rows(normed, shared_u).astype(jnp.bfloat16),
    )
    gate_part, up_part, sgate_part, sup_part = tuple(
        (
            part.astype(jnp.float32)
            for part in in_one_piece(
                (partials[0], partials[1], partials[2], partials[3]), "tp", 1, 0
            )
        )
    )
    hidden, shared_hidden = (
        lax.all_gather(
            (jax.nn.silu(gate_part) * up_part).astype(jnp.bfloat16), "tp", axis=1, tiled=True
        ),
        lax.all_gather(
            (jax.nn.silu(sgate_part) * sup_part).astype(jnp.bfloat16), "tp", axis=1, tiled=True
        ),
    )
    produced = jnp.dot(hidden, down_new[0], preferred_element_type=jnp.float32).astype(jnp.bfloat16)
    returned = lax.all_to_all(
        produced.reshape(experts, capacity, portion_width),
        "fs",
        split_axis=0,
        concat_axis=0,
        tiled=True,
    )
    picked = returned.reshape(experts * capacity, portion_width)[target]
    routed = jnp.sum(routing_weight[:, :, None] * picked.astype(jnp.float32), axis=1)
    shared_out = jnp.dot(shared_hidden, shared_d, preferred_element_type=jnp.float32)
    mixed = (routed + shared_out).astype(jnp.bfloat16)
    return (mixed, gate_refreshed, up_new, down_new, shared_g, shared_u, shared_d)


def solution(mesh):
    return jax.shard_map(
        per_device,
        mesh=mesh,
        in_specs=(
            P(("grp", "fs"), "tp"),
            P(("grp", "fs"), None),
            P(("grp", "fs"), None),
            P("tp"),
            P(None, "fs", "tp"),
            P(None, "fs", "tp"),
            P(None, "fs", "tp"),
            P("fs", "tp"),
            P("fs", "tp"),
            P("fs", "tp"),
        ),
        out_specs=(
            P(("grp", "fs"), "tp"),
            P(("grp", "fs"), None, "tp"),
            P(("grp", "fs"), None, "tp"),
            P(("grp", "fs"), None, "tp"),
            P("grp", "tp"),
            P("grp", "tp"),
            P("grp", "tp"),
        ),
        check_vma=False,
    )
```

profile of v0, /device:TPU:33, one launch (start us, length us, event | category | flops | bytes accessed | tf_op | source)
XLA Modules:
  0.0 525.0 jit_solution(1667189688354686824)
XLA Ops:
  7.2 1.1 convert_element_type.88
  8.3 1.3 multiply_convert_fusion.1
  9.6 0.0 copy-start.8
  9.6 1.0 pad_maximum_fusion.1
  10.6 46.3 %all-to-all-start.1 = ((bf16[32,16,768]{2,1,0:T(8,128)(2,1)}), bf16[32,16,768]{2,1,0:T(8,128)(2,1)S(1)}, u32[]{:S(2)}, u32[]{:S(2)}) async-start(bf16[32,16,768]{2,1,0:T(8,128)(2,1)} %pad_maximum_fusion.1), calls=%async_computation.1 | async-start | bytes 1572864 | tf_op jit(solution)/shard_map/all_to_all | solution.py:12
  56.9 0.0 copy-start
  56.9 0.1 copy.45
  57.0 0.1 eq.42
  57.1 0.1 eq.38
  57.3 9.1 %reduce-window.6 = s32[32,12,128]{2,1,0:T(8,128)S(1)} reduce-window(s32[32,12,128]{2,1,0:T(8,128)S(1)} %fusion.11, s32[]{:T(128)} %constant.6.clone.1), window={size=1x1x128 pad=0_0x0_0x127_0}, to_apply=%region_0.0 | reduce-window | flops 6242304 | bytes 393220 | tf_op jit(solution)/shard_map/reduce-window
  66.4 0.1 slice.38
  66.5 0.2 copy.47
  66.7 0.1 copy.48
  66.8 0.1 broadcast_add_fusion
  66.9 0.1 fusion.16
  67.0 0.1 reduce_sum.39
  67.1 0.1 copy.49
  67.2 0.1 copy.50
  67.3 0.1 fusion.12
  67.5 13.3 %psum.7 = f32[192]{0:T(256)S(1)} all-reduce(f32[192]{0:T(256)S(1)} %fusion.12), channel_id=1, replica_groups=mesh['grp'=2,'fs'=32,'tp'=8] {'tp'}, use_global_device_ids=true, to_apply=%region_5.6 | all-reduce | flops 192 | bytes 1536 | tf_op jit(solution)/shard_map/psum | solution.py:74
  80.8 5.0 convert_reduce_fusion
  85.8 0.0 copy-start.11
  85.8 0.0 copy-start.9
  85.8 0.0 copy-start.10
  85.9 0.0 copy-start.13
  85.9 1.5 convolution_convert_fusion.3
  87.3 55.5 %all-to-all-done.1 = bf16[32,16,768]{2,1,0:T(8,128)(2,1)S(1)} async-done(((bf16[32,16,768]{2,1,0:T(8,128)(2,1)}), bf16[32,16,768]{2,1,0:T(8,128)(2,1)S(1)}, u32[]{:S(2)}, u32[]{:S(2)}) %all-to-all-start.1) | async-done | bytes 786464 | tf_op jit(solution)/shard_map/all_to_all | solution.py:12
  142.8 4.8 all-to-all-start
  147.7 0.1 reduce-scatter.4.cloned.1.call-start
  147.8 0.0 copy-done.11
  147.8 122.6 %all_gather.9 = bf16[512,768]{1,0:T(8,128)(2,1)S(1)} all-gather(bf16[16,768]{1,0:T(8,128)(2,1)S(1)} %pad_maximum_fusion.2), channel_id=1, replica_groups=mesh['grp'=2,'fs'=32,'tp'=8] {'fs'}, dimensions={0}, use_global_device_ids=true | all-gather | bytes 811008 | tf_op jit(solution)/shard_map/all_gather | solution.py:18
  270.4 0.1 fusion.25
  270.5 0.0 copy-start.4
  270.5 0.0 copy-start.5
  270.5 0.0 copy-start.1
  270.5 0.2 convolution_convert_fusion.4
  270.7 0.9 convolution_convert_fusion.5
  271.7 0.1 fusion.26
  271.7 0.0 copy-start.2
  271.7 0.0 copy-start.3
  271.8 0.0 copy-start.7
  271.8 0.0 all-to-all-done
  271.8 0.7 convolution_convert_fusion
  272.5 0.7 convolution_convert_fusion.1
  273.2 0.2 copy-done.6
  273.4 2.1 pad_maximum_fusion
  275.5 6.3 %copy.56 = bf16[3968,512]{0,1:T(8,128)(2,1)} copy(bf16[3968,512]{1,0:T(8,128)(2,1)} %pad_maximum_fusion) | data formatting | bytes 8126464
  281.8 0.1 reduce-scatter.4.cloned.1.call-update
  281.8 0.2 all-gather.2.cloned.1.call-start
  282.1 64.3 %reduce-scatter.4.cloned.1.call-done = bf16[64,3968]{1,0:T(8,128)(2,1)} async-done(((bf16[512,3968]{1,0:T(8,128)(2,1)}), bf16[64,3968]{1,0:T(8,128)(2,1)}) %reduce-scatter.4.cloned.1.call-update) | async-done | bytes 507920
  346.4 1.9 fusion.7
  348.3 0.1 all-gather.2.cloned.1.call-update
  348.3 41.7 %all-gather.2.cloned.1.call-done = bf16[1792,512]{0,1:T(8,128)(2,1)} async-done(((bf16[1792,64]{0,1:T(8,128)(2,1)}), bf16[1792,512]{0,1:T(8,128)(2,1)}) %all-gather.2.cloned.1.call-update) | async-done | bytes 1835024 | tf_op jit(solution)/shard_map/all_gather | solution.py:113
  390.0 3.1 convolution_convert_fusion.2
  393.1 23.3 %all-to-all-start.2 = ((bf16[32,56,256]{2,1,0:T(8,128)(2,1)}), bf16[32,56,256]{2,1,0:T(8,128)(2,1)S(1)}, u32[]{:S(2)}, u32[]{:S(2)}) async-start(bf16[32,56,256]{2,1,0:T(8,128)(2,1)} %bitcast.8), calls=%async_computation.2 | async-start | bytes 1835008 | tf_op jit(solution)/shard_map/all_to_all | solution.py:121
  416.5 0.1 copy.53
  416.6 0.1 reshape.66
  416.7 0.1 copy.44
  416.8 0.9 fusion.21
  417.7 13.4 %all_gather.11 = bf16[192,512]{0,1:T(8,128)(2,1)S(1)} all-gather(bf16[192,64]{0,1:T(8,128)(2,1)S(1)} %fusion.21), channel_id=1, replica_groups=mesh['grp'=2,'fs'=32,'tp'=8] {'tp'}, dimensions={1}, use_global_device_ids=true | all-gather | bytes 221184 | tf_op jit(solution)/shard_map/all_gather | solution.py:116
  431.2 80.7 %all-to-all-done.2 = bf16[32,56,256]{2,1,0:T(8,128)(2,1)S(1)} async-done(((bf16[32,56,256]{2,1,0:T(8,128)(2,1)}), bf16[32,56,256]{2,1,0:T(8,128)(2,1)S(1)}, u32[]{:S(2)}, u32[]{:S(2)}) %all-to-all-start.2) | async-done | bytes 917536 | tf_op jit(solution)/shard_map/all_to_all | solution.py:121
  511.9 4.8 gather_fusion
  516.7 0.5 fusion
  517.2 0.9 fusion.1
  (22 shorter events, 0.1 us)
Async XLA Ops:
  9.6 47.3 %copy-start.8 = (s32[192,8]{0,1:T(8,128)S(1)}, s32[192,8]{0,1:T(8,128)}, u32[]{:S(2)}) copy-start(s32[192,8]{0,1:T(8,128)} %param.11) | copy-start | bytes 18436
  10.6 132.3 %all-to-all-start.1 = ((bf16[32,16,768]{2,1,0:T(8,128)(2,1)}), bf16[32,16,768]{2,1,0:T(8,128)(2,1)S(1)}, u32[]{:S(2)}, u32[]{:S(2)}) async-start(bf16[32,16,768]{2,1,0:T(8,128)(2,1)} %pad_maximum_fusion.1), calls=%async_computation.1 | async-start | bytes 1572864 | tf_op jit(solution)/shard_map/all_to_all | solution.py:12
  56.9 10.4 %copy-start = (bf16[192,256]{1,0:T(8,128)(2,1)S(1)}, bf16[192,256]{1,0:T(8,128)(2,1)}, u32[]{:S(2)}) copy-start(bf16[192,256]{1,0:T(8,128)(2,1)} %param.10) | copy-start | bytes 294916
  85.8 61.9 %copy-start.11 = (f32[16,256]{1,0:T(8,128)S(1)}, f32[16,256]{1,0:T(8,128)}, u32[]{:S(2)}) copy-start(f32[16,256]{1,0:T(8,128)} %param.19) | copy-start | bytes 49156
  85.8 62.0 %copy-start.9 = (f32[16,256]{1,0:T(8,128)S(1)}, f32[16,256]{1,0:T(8,128)}, u32[]{:S(2)}) copy-start(f32[16,256]{1,0:T(8,128)} %param.17) | copy-start | bytes 49156
  85.8 62.0 %copy-start.10 = (f32[16,256]{1,0:T(8,128)S(1)}, f32[16,256]{1,0:T(8,128)}, u32[]{:S(2)}) copy-start(f32[16,256]{1,0:T(8,128)} %param.18) | copy-start | bytes 49156
  85.9 62.0 %copy-start.13 = (f32[256]{0:T(256)S(1)}, f32[256]{0:T(256)}, u32[]{:S(2)}) copy-start(f32[256]{0:T(256)} %param.13) | copy-start | bytes 3076
  142.8 128.9 %all-to-all-start = ((bf16[32,56,256]{2,1,0:T(8,128)(2,1)}), bf16[32,56,256]{2,1,0:T(8,128)(2,1)S(1)}, u32[]{:S(2)}, u32[]{:S(2)}) async-start(bf16[32,56,256]{2,1,0:T(8,128)(2,1)} %bitcast.2), calls=%async_computation | async-start | bytes 1835008 | tf_op jit(solution)/shard_map/all_to_all | solution.py:90
  147.7 198.7 %reduce-scatter.4.cloned.1.call-start = ((), (), s32[]{:S(2)}) async-start(), calls=%async_computation.5 | async-start | bytes 4571136
  270.5 2.0 copy-start.4
  270.5 2.0 copy-start.5
  270.5 246.7 %copy-start.1 = (bf16[512,256]{1,0:T(8,128)(2,1)}, bf16[512,256]{1,0:T(8,128)(2,1)S(1)}, u32[]{:S(2)}) copy-start(bf16[512,256]{1,0:T(8,128)(2,1)S(1)} %get-tuple-element.9) | copy-start | bytes 786436
  271.7 1.4 copy-start.2
  271.7 1.4 copy-start.3
  271.8 118.2 %copy-start.7 = (bf16[1,512,256]{2,1,0:T(8,128)(2,1)}, bf16[1,512,256]{2,1,0:T(8,128)(2,1)S(1)}, u32[]{:S(2)}) copy-start(bf16[1,512,256]{2,1,0:T(8,128)(2,1)S(1)} %get-tuple-element.12) | copy-start | bytes 786436
  272.5 0.9 copy-start.6
  281.8 108.2 %all-gather.2.cloned.1.call-start = ((), (), s32[]{:S(2)}) async-start(), calls=%async_computation.4 | async-start | bytes 2064384 | tf_op jit(solution)/shard_map/all_gather | solution.py:113
  393.1 23.6 %copy-start.12 = (f32[192,8]{0,1:T(8,128)S(1)}, f32[192,8]{0,1:T(8,128)}, u32[]{:S(2)}) copy-start(f32[192,8]{0,1:T(8,128)} %param.12) | copy-start | bytes 18436
  393.1 118.8 %all-to-all-start.2 = ((bf16[32,56,256]{2,1,0:T(8,128)(2,1)}), bf16[32,56,256]{2,1,0:T(8,128)(2,1)S(1)}, u32[]{:S(2)}, u32[]{:S(2)}) async-start(bf16[32,56,256]{2,1,0:T(8,128)(2,1)} %bitcast.8), calls=%async_computation.2 | async-start | bytes 1835008 | tf_op jit(solution)/shard_map/all_to_all | solution.py:121
Sparse Core Ops, SparseCore 0:
  281.9 64.3 reduce-scatter.3
  348.5 41.4 all-gather.1
where the time goes:
time: 526 us; the launch traced here: 525 us
  waiting for transfers between devices  242 us (46%)
  blocking collectives  149 us (28%)
  starting transfers between devices  74.8 us (14%)
  other arithmetic  23.3 us (4%)
  between operations  14.5 us (3%)
  local copies, waits for them, and re-layouts  12.8 us (2%)
  matrix products  8.01 us (2%)
    all_gather x1, blocking collectives, sent_together_2(): out, at, outs = (lax.all_gather(both, axis, axis=dim, tiled=True), 0, [])  123 us
    all_to_all x1, waiting for transfers between devices, per_device(): lax.all_to_all(produced.reshape(experts, capacity, portion_width), 'fs',...  80.7 us
    unnamed x3, waiting for transfers between devices  64.4 us
    all_to_all x1, waiting for transfers between devices, sent_together(): lax.all_to_all(both, axis, split_axis=split_dim, concat_axis=concat_dim,...  55.5 us
    all_to_all x1, starting transfers between devices, sent_together(): lax.all_to_all(both, axis, split_axis=split_dim, concat_axis=concat_dim,...  46.3 us
    all_gather x1, waiting for transfers between devices, per_device(): lax.all_gather((jax.nn.silu(gate_part) * up_part).astype(jnp.bfloat16), '...  41.7 us
    all_to_all x1, starting transfers between devices, per_device(): lax.all_to_all(produced.reshape(experts, capacity, portion_width), 'fs',...  23.3 us
    all_gather x1, blocking collectives, per_device(): lax.all_gather((jax.nn.silu(sgate_part) * sup_part).astype(jnp.bfloat16),...  13.4 us
  transfers between devices with their start and end apart: 5, of which 4 were waited for; matrix products, arithmetic and copies ran while one was open for 4% of the time, Pallas kernels for 0%

commit v1 on v0

v1 whole, which is shorter than its diff:
```python
import functools

import jax
import jax.numpy as jnp
from jax import lax
from jax.experimental import pallas as pl
from jax.experimental.pallas import tpu as pltpu
from jax.sharding import PartitionSpec as P

norm_eps = 1e-06


def rows_dot(rows, weight):
    return lax.dot_general(
        rows, weight, (((1,), (1,)), ((), ())), preferred_element_type=jnp.float32
    )


def mlp_kernel(parts, hidden_units, x_ref, gu_ref, down_ref, out_ref, acc, hidden):
    step = pl.program_id(0)

    @pl.when(step == 0)
    def _():
        acc[...] = jnp.zeros_like(acc)

    @pl.when(step < parts)
    def _():
        acc[...] += rows_dot(x_ref[0], gu_ref[0])

    @pl.when(step == parts - 1)
    def _():
        gate = acc[:, :hidden_units]
        up = acc[:, hidden_units:]
        hidden[...] = (gate / (1.0 + jnp.exp(-gate)) * up).astype(jnp.bfloat16)

    @pl.when(step >= parts)
    def _():
        out_ref[0] = jnp.dot(
            hidden[...], down_ref[0], preferred_element_type=jnp.float32
        ).astype(jnp.bfloat16)


def expert_mlp(x, weights):
    parts, rows, width = x.shape
    units = weights.shape[1] // 3
    return pl.pallas_call(
        functools.partial(mlp_kernel, parts, units),
        grid=(2 * parts,),
        in_specs=[
            pl.BlockSpec((1, rows, width), lambda i: (jnp.minimum(i, parts - 1), 0, 0)),
            pl.BlockSpec((1, 2 * units, width), lambda i: (jnp.minimum(i, parts - 1), 0, 0)),
            pl.BlockSpec((1, units, width), lambda i: (jnp.maximum(i - parts, 0), 2, 0)),
        ],
        out_specs=pl.BlockSpec((1, rows, width), lambda i: (jnp.maximum(i - parts, 0), 0, 0)),
        out_shape=jax.ShapeDtypeStruct((parts, rows, width), jnp.bfloat16),
        scratch_shapes=[
            pltpu.VMEM((rows, 2 * units), jnp.float32),
            pltpu.VMEM((rows, units), jnp.bfloat16),
        ],
        cost_estimate=pl.CostEstimate(
            flops=6 * parts * rows * units * width,
            bytes_accessed=2 * (2 * x.size + weights.size),
            transcendentals=rows * units,
        ),
        name="expert_mlp",
    )(x, weights, weights)


def layer(
    tokens,
    routes,
    routing_weight,
    norm_gain_vector,
    expert_gate,
    expert_up,
    expert_down,
    shared_gate,
    shared_up,
    shared_down,
):
    tok_rows, width = tokens.shape
    groups, places, parts = (lax.axis_size(a) for a in ("grp", "fs", "tp"))
    model_width = width * parts
    experts, unit_rows, _ = expert_gate.shape
    top_count = routes.shape[1]
    capacity = tok_rows * top_count * 7 // (6 * experts)
    own = unit_rows // groups
    first = lax.axis_index("grp") * own

    gain = norm_gain_vector[None, None, :]

    def share(w):
        return lax.dynamic_slice_in_dim(w, first, own, axis=w.ndim - 2)

    def spread(w):
        return jnp.broadcast_to(share(w)[None], (experts, own, width))

    pieces = [
        (share(expert_gate) * gain).astype(jnp.bfloat16),
        (share(expert_up) * gain).astype(jnp.bfloat16),
        share(expert_down).astype(jnp.bfloat16),
        (spread(shared_gate) * gain).astype(jnp.bfloat16),
        (spread(shared_up) * gain).astype(jnp.bfloat16),
        spread(shared_down).astype(jnp.bfloat16),
    ]
    got = lax.all_to_all(
        jnp.concatenate(pieces, axis=1), "fs", split_axis=0, concat_axis=0, tiled=True
    )
    got = lax.all_gather(got, "grp", axis=0, tiled=False)
    got = got.reshape(groups, places, 6, own, width).transpose(2, 1, 0, 3, 4)
    units = places * groups * own
    got = got.reshape(6, units, width)
    gate_new, up_new, down_new, shared_g, shared_u, shared_d = (got[i] for i in range(6))
    whole = lax.all_gather(got[:3].reshape(3 * units, width), "tp", axis=0, tiled=False)

    values = tokens.astype(jnp.float32)
    totals = lax.psum(jnp.sum(values * values, axis=1), "tp")
    normed = (values * lax.rsqrt(totals / model_width + norm_eps)[:, None]).astype(jnp.bfloat16)
    named = routes.T[:, None, :] == jnp.arange(experts, dtype=jnp.int32)[None, :, None]
    member = jnp.any(named, axis=0)
    weight = jnp.sum(jnp.where(named, routing_weight.T[:, None, :], 0.0), axis=0)
    spot = jnp.arange(tok_rows, dtype=jnp.int32)
    before = (spot[:, None] < spot[None, :]).astype(jnp.bfloat16)
    slot = jnp.dot(
        member.astype(jnp.bfloat16), before, preferred_element_type=jnp.float32
    ).astype(jnp.int32)
    slot = jnp.where(member, slot, -1)
    placed = slot[:, None, :] == jnp.arange(capacity, dtype=jnp.int32)[None, :, None]
    placing = placed.astype(jnp.bfloat16).reshape(experts * capacity, tok_rows)
    high = lax.reduce_precision(weight, 8, 7)
    low = weight - high

    def weighted(w):
        return jnp.where(placed, w[:, None, :], 0.0).astype(jnp.bfloat16).reshape(
            experts * capacity, tok_rows
        )

    outgoing = jnp.dot(placing, normed, preferred_element_type=jnp.float32)
    outgoing = outgoing.astype(jnp.bfloat16).reshape(experts, capacity, width)
    incoming = lax.all_to_all(outgoing, "fs", split_axis=0, concat_axis=0, tiled=True)
    chunk = places * capacity // parts
    gathered = lax.all_to_all(
        incoming.reshape(parts, chunk, width), "tp", split_axis=0, concat_axis=0, tiled=True
    )
    produced = expert_mlp(gathered, whole)
    produced = lax.all_to_all(produced, "tp", split_axis=0, concat_axis=0, tiled=True)
    returned = lax.all_to_all(
        produced.reshape(places, capacity, width), "fs", split_axis=0, concat_axis=0, tiled=True
    )
    returned = returned.reshape(experts * capacity, width)

    share_units = units // parts
    both = jnp.concatenate(
        [shared_g.reshape(parts, share_units, width), shared_u.reshape(parts, share_units, width)],
        axis=1,
    ).reshape(2 * units, width)
    partial = rows_dot(normed, both).astype(jnp.bfloat16)
    sums = lax.psum_scatter(
        partial.reshape(tok_rows, parts, 2 * share_units).transpose(1, 0, 2),
        "tp",
        scatter_dimension=0,
        tiled=False,
    ).astype(jnp.float32)
    shared_hidden = (jax.nn.silu(sums[:, :share_units]) * sums[:, share_units:]).astype(
        jnp.bfloat16
    )
    shared_hidden = lax.all_gather(shared_hidden, "tp", axis=1, tiled=True)
    shared_out = jnp.dot(shared_hidden, shared_d, preferred_element_type=jnp.float32)

    def taken(w):
        return lax.dot_general(
            weighted(w), returned, (((0,), (0,)), ((), ())), preferred_element_type=jnp.float32
        )

    mixed = (taken(high) + taken(low) + shared_out).astype(jnp.bfloat16)
    return (
        mixed,
        gate_new[None],
        up_new[None],
        down_new[None],
        shared_g,
        shared_u,
        shared_d,
    )


def solution(mesh):
    return jax.shard_map(
        layer,
        mesh=mesh,
        in_specs=(
            P(("grp", "fs"), "tp"),
            P(("grp", "fs"), None),
            P(("grp", "fs"), None),
            P("tp"),
            P(None, "fs", "tp"),
            P(None, "fs", "tp"),
            P(None, "fs", "tp"),
            P("fs", "tp"),
            P("fs", "tp"),
            P("fs", "tp"),
        ),
        out_specs=(
            P(("grp", "fs"), "tp"),
            P(("grp", "fs"), None, "tp"),
            P(("grp", "fs"), None, "tp"),
            P(("grp", "fs"), None, "tp"),
            P("grp", "tp"),
            P("grp", "tp"),
            P("grp", "tp"),
        ),
        check_vma=False,
    )
```

time: 526 us -> 472 us (0.90)
  blocking collectives: 149 us -> 316 us
  waiting for transfers between devices: 242 us -> 105 us
  starting transfers between devices: 74.8 us -> 5.03 us
  other arithmetic: 23.3 us -> 3.94 us
  Pallas kernels: 0 us -> 12.1 us
    all_to_all x0 -> x4, blocking collectives: none -> 290 us  [the longest x1 132 us: layer(): lax.all_to_all(jnp.concatenate(pieces, axis=1), 'fs', split_axis=0, conca...]
    all_gather x2 -> x1, blocking collectives: 136 us -> 13.9 us  [layer(): shared_hidden = lax.all_gather(shared_hidden, 'tp', axis=1, tiled=True)]
    all_to_all x3 -> x1, waiting for transfers between devices: 136 us -> 31.5 us  [layer(): lax.all_to_all(produced.reshape(places, capacity, width), 'fs', split_axi...]
    all_to_all x3 -> x1, starting transfers between devices: 74.5 us -> 4.84 us  [layer(): lax.all_to_all(produced.reshape(places, capacity, width), 'fs', split_axi...]
    unnamed x3, waiting for transfers between devices: 64.4 us -> 0.16 us
    reduce_scatter x0 -> x1, waiting for transfers between devices: none -> 44 us  [layer(): lax.psum_scatter(partial.reshape(tok_rows, parts, 2 * share_units).transp...]
    all_gather x1 -> x2, waiting for transfers between devices: 41.7 us -> 29.2 us  [the longest x1 29.2 us: layer(): got = lax.all_gather(got, 'grp', axis=0, tiled=False)]
    pallas_call x0 -> x1, Pallas kernels: none -> 12.1 us  [expert_mlp(): pl.pallas_call(functools.partial(mlp_kernel, parts, units), grid=(2 * par...]
  transfers between devices with their start and end apart: 5 -> 4, of which waited for: 4 -> 3; matrix products, arithmetic and copies ran while one was open for 4% -> 1% of each run, Pallas kernels for 0% -> 0%
where the time goes in v1:
time: 472 us; the launch traced here: 469 us
  blocking collectives  316 us (67%)
  waiting for transfers between devices  105 us (22%)
  between operations  14.1 us (3%)
  Pallas kernels  12.1 us (3%)
  local copies, waits for them, and re-layouts  9.84 us (2%)
  starting transfers between devices  5.03 us (1%)
    all_to_all x1, blocking collectives, layer(): lax.all_to_all(jnp.concatenate(pieces, axis=1), 'fs', split_axis=0, conca...  132 us
    all_to_all x1, blocking collectives, layer(): lax.all_to_all(outgoing, 'fs', split_axis=0, concat_axis=0, tiled=True)  117 us
    reduce_scatter x1, waiting for transfers between devices, layer(): lax.psum_scatter(partial.reshape(tok_rows, parts, 2 * share_units).transp...  44 us
    all_to_all x1, waiting for transfers between devices, layer(): lax.all_to_all(produced.reshape(places, capacity, width), 'fs', split_axi...  31.5 us
    all_gather x1, waiting for transfers between devices, layer(): got = lax.all_gather(got, 'grp', axis=0, tiled=False)  29.2 us
    all_to_all x1, blocking collectives, layer(): lax.all_to_all(incoming.reshape(parts, chunk, width), 'tp', split_axis=0,...  21.5 us
    all_to_all x1, blocking collectives, layer(): lax.all_to_all(produced, 'tp', split_axis=0, concat_axis=0, tiled=True)  19 us
    all_gather x1, blocking collectives, layer(): shared_hidden = lax.all_gather(shared_hidden, 'tp', axis=1, tiled=True)  13.9 us
  transfers between devices with their start and end apart: 4, of which 3 were waited for; matrix products, arithmetic and copies ran while one was open for 1% of the time, Pallas kernels for 0%

profile of v1, /device:TPU:33, one launch (start us, length us, event | category | flops | bytes accessed | tf_op | source)
XLA Modules:
  0.0 468.9 jit_solution(10791497337544878989)
XLA Ops:
  7.2 0.0 copy-start
  7.2 0.1 all-gather.6.cloned.1.call-start
  7.3 0.6 copy-done
  7.9 1.0 fusion.13
  8.9 1.0 fusion.14
  9.9 1.0 fusion.15
  10.8 0.7 constant_dynamic-slice_fusion
  11.6 0.7 fusion.16
  12.3 0.7 fusion.17
  13.0 132.1 %all_to_all.25 = bf16[32,48,256]{2,1,0:T(8,128)(2,1)} all-to-all(bf16[32,48,256]{2,1,0:T(8,128)(2,1)S(1)} %broadcast_dynamic-update-slice_fusion), channel_id=1, replica_groups=mesh['grp'=2,'fs'=32,'tp'=8] {'fs'}, dimensions={0} | all-to-all | bytes 1572864 | tf_op jit(solution)/shard_map/all_to_all | solution.py:106
  145.1 0.1 all-gather.6.cloned.1.call-update
  145.2 0.1 all-gather.4.cloned.1.call-start
  145.2 29.2 %all-gather.6.cloned.1.call-done = bf16[64,48,256]{2,1,0:T(8,128)(2,1)} async-done(((bf16[32,48,256]{2,1,0:T(8,128)(2,1)}), bf16[64,48,256]{2,1,0:T(8,128)(2,1)}) %all-gather.6.cloned.1.call-update) | async-done | bytes 1572880 | tf_op jit(solution)/shard_map/all_gather | solution.py:109
  174.5 0.0 copy-start.7
  174.5 1.2 slice.52
  175.7 0.0 copy-start.5
  175.7 1.0 copy.55
  176.7 0.1 all-gather.4.cloned.1.call-update
  176.8 0.1 eq.45
  176.9 0.0 copy-done.7
  176.9 0.1 fusion.3
  177.1 0.3 bitcast_compare_fusion
  177.4 0.3 copy-done.9
  177.7 0.0 copy-done.5
  177.7 0.1 fusion.11
  177.8 12.7 %psum.7 = f32[192]{0:T(256)S(1)} all-reduce(f32[192]{0:T(256)S(1)} %fusion.11), channel_id=1, replica_groups=mesh['grp'=2,'fs'=32,'tp'=8] {'tp'}, use_global_device_ids=true, to_apply=%region_3.4 | all-reduce | flops 192 | bytes 1536 | tf_op jit(solution)/shard_map/psum | solution.py:117
  190.5 0.5 convolution_convert_fusion
  191.0 117.1 %all_to_all.26 = bf16[32,56,256]{2,1,0:T(8,128)(2,1)S(1)} all-to-all(bf16[32,56,256]{2,1,0:T(8,128)(2,1)S(1)} %bitcast.44), channel_id=1, replica_groups=mesh['grp'=2,'fs'=32,'tp'=8] {'fs'}, dimensions={0} | all-to-all | bytes 1835008 | tf_op jit(solution)/shard_map/all_to_all | solution.py:140
  308.0 0.0 copy-done.11
  308.1 21.5 %all_to_all.27.x_ref = bf16[8,224,256]{2,1,0:T(8,128)(2,1)} all-to-all(bf16[8,224,256]{2,1,0:T(8,128)(2,1)S(1)} %bitcast.45), channel_id=1, replica_groups=mesh['grp'=2,'fs'=32,'tp'=8] {'tp'}, dimensions={0} | all-to-all | bytes 1835008 | tf_op jit(solution)/shard_map/all_to_all | solution.py:142
  329.5 12.1 %expert_mlp.1 = bf16[8,224,256]{2,1,0:T(8,128)(2,1)} custom-call(bf16[8,224,256]{2,1,0:T(8,128)(2,1)} %all_to_all.27.x_ref, bf16[8,1536,256]{2,1,0:T(8,128)(2,1)} %all-gather.4.cloned.1.call-done.gu_ref.down_ref, bf16[8,1536,256]{2,1,0:T(8,128)(2,1)} %all-gather.4.cloned.1.call-done.gu_ref.down_ref), custom_call_target="tpu_custom_call" | custom-call | flops 1409286144 | bytes 8126464 | tf_op jit(solution)/shard_map/expert_mlp/pallas_call | solution.py:46
  341.6 19.0 %all_to_all.28 = bf16[8,224,256]{2,1,0:T(8,128)(2,1)} all-to-all(bf16[8,224,256]{2,1,0:T(8,128)(2,1)} %expert_mlp.1), channel_id=1, replica_groups=mesh['grp'=2,'fs'=32,'tp'=8] {'tp'}, dimensions={0} | all-to-all | bytes 1835008 | tf_op jit(solution)/shard_map/all_to_all | solution.py:146
  360.6 4.8 %all-to-all-start.4 = ((bf16[32,56,256]{2,1,0:T(8,128)(2,1)}), bf16[32,56,256]{2,1,0:T(8,128)(2,1)S(1)}, u32[]{:S(2)}, u32[]{:S(2)}) async-start(bf16[32,56,256]{2,1,0:T(8,128)(2,1)} %bitcast.8), calls=%async_computation.4 | async-start | bytes 1835008 | tf_op jit(solution)/shard_map/all_to_all | solution.py:147
  365.4 0.1 reduce-scatter.2.cloned.1.call-start
  365.5 0.0 copy-done.1
  365.5 0.1 fusion.23
  365.6 0.0 copy-start.6
  365.6 0.0 copy-start.12
  365.7 0.0 copy-start.3
  365.7 0.0 copy-start.8
  365.7 0.0 copy-start.13
  365.7 0.0 copy-start.4
  365.8 0.7 copy-done.6
  366.5 0.0 copy-done.12
  366.5 0.3 fusion
  366.8 0.8 copy.68
  367.7 0.1 reduce-scatter.2.cloned.1.call-update
  367.7 0.0 copy-done.3
  367.7 0.0 copy-done.8
  367.8 0.0 copy-done.13
  367.9 0.0 copy-done.4
  367.9 0.0 copy-start.2
  367.9 0.8 copy.61
  368.7 0.7 copy.62
  369.4 0.7 copy.63
  370.1 44.0 %reduce-scatter.2.cloned.1.call-done = bf16[1,192,128]{2,1,0:T(8,128)(2,1)} async-done(((bf16[8,192,128]{2,1,0:T(8,128)(2,1)}), bf16[1,192,128]{2,1,0:T(8,128)(2,1)}) %reduce-scatter.2.cloned.1.call-update) | async-done | bytes 49168 | tf_op jit(solution)/shard_map/reduce_scatter | solution.py:158
  414.1 0.9 copy.59
  415.1 13.9 %all_gather.15 = bf16[192,512]{0,1:T(8,128)(2,1)S(1)} all-gather(bf16[192,64]{0,1:T(8,128)(2,1)S(1)} %fusion.18), channel_id=1, replica_groups=mesh['grp'=2,'fs'=32,'tp'=8] {'tp'}, dimensions={1}, use_global_device_ids=true | all-gather | bytes 221184 | tf_op jit(solution)/shard_map/all_gather | solution.py:167
  428.9 31.5 %all-to-all-done.4 = bf16[32,56,256]{2,1,0:T(8,128)(2,1)S(1)} async-done(((bf16[32,56,256]{2,1,0:T(8,128)(2,1)}), bf16[32,56,256]{2,1,0:T(8,128)(2,1)S(1)}, u32[]{:S(2)}, u32[]{:S(2)}) %all-to-all-start.4) | async-done | bytes 917536 | tf_op jit(solution)/shard_map/all_to_all | solution.py:147
  460.4 0.0 copy-done.10
  460.5 0.5 convolution_bitcast_fusion
  460.9 0.5 fusion.1
  461.4 0.0 copy-done.2
  461.4 0.9 fusion.2
  (18 shorter events, 0.3 us)
Async XLA Ops:
  7.2 0.7 copy-start
  7.2 167.3 %all-gather.6.cloned.1.call-start = ((), (), s32[]{:S(2)}) async-start(), calls=%async_computation.8 | async-start | bytes 2359296 | tf_op jit(solution)/shard_map/all_gather | solution.py:109
  145.2 184.3 %all-gather.4.cloned.1.call-start = ((), (), s32[]{:S(2)}) async-start(), calls=%async_computation.6 | async-start | bytes 7077888 | tf_op jit(solution)/shard_map/all_gather | solution.py:114
  174.5 2.4 copy-start.7
  175.7 2.0 copy-start.5
  177.1 0.6 copy-start.9
  190.5 117.6 %copy-start.11 = (f32[192]{0:T(256)}, f32[192]{0:T(256)S(1)}, u32[]{:S(2)}) copy-start(f32[192]{0:T(256)S(1)} %add_rsqrt_fusion) | copy-start | bytes 2308
  341.6 23.9 %copy-start.1 = (bf16[64,48,256]{2,1,0:T(8,128)(2,1)S(1)}, bf16[64,48,256]{2,1,0:T(8,128)(2,1)}, u32[]{:S(2)}) copy-start(bf16[64,48,256]{2,1,0:T(8,128)(2,1)} %all-gather.6.cloned.1.call-done) | copy-start | bytes 4718596
  360.6 99.9 %all-to-all-start.4 = ((bf16[32,56,256]{2,1,0:T(8,128)(2,1)}), bf16[32,56,256]{2,1,0:T(8,128)(2,1)S(1)}, u32[]{:S(2)}, u32[]{:S(2)}) async-start(bf16[32,56,256]{2,1,0:T(8,128)(2,1)} %bitcast.8), calls=%async_computation.4 | async-start | bytes 1835008 | tf_op jit(solution)/shard_map/all_to_all | solution.py:147
  365.4 48.7 %reduce-scatter.2.cloned.1.call-start = ((), (), s32[]{:S(2)}) async-start(), calls=%async_computation.7 | async-start | bytes 442368 | tf_op jit(solution)/shard_map/reduce_scatter | solution.py:158
  365.6 0.9 copy-start.6
  365.6 0.9 copy-start.12
  365.7 2.1 copy-start.3
  365.7 2.1 copy-start.8
  365.7 2.1 copy-start.13
  365.7 2.1 copy-start.4
  367.7 92.8 %copy-start.10 = (s32[32,192]{1,0:T(8,128)S(1)}, s32[32,192]{1,0:T(8,128)}, u32[]{:S(2)}) copy-start(s32[32,192]{1,0:T(8,128)} %copy-done.9) | copy-start | bytes 73732
  367.9 93.6 %copy-start.2 = (bf16[1,32,2,8,256]{4,3,2,1,0:T(8,128)(2,1)}, bf16[1,32,2,8,256]{4,3,2,1,0:T(8,128)(2,1)S(1)}, u32[]{:S(2)}) copy-start(bf16[1,32,2,8,256]{4,3,2,1,0:T(8,128)(2,1)S(1)} %copy.60) | copy-start | bytes 786436
Sparse Core Ops, SparseCore 0:
  145.3 29.1 all-gather.5
  176.9 58.1 all-gather.3
  369.1 44.9 reduce-scatter.1

commit v2 on v1

v2 whole, which is shorter than its diff:
```python
import functools

import jax
import jax.numpy as jnp
from jax import lax
from jax.experimental import pallas as pl
from jax.experimental.pallas import tpu as pltpu
from jax.sharding import PartitionSpec as P

norm_eps = 1e-06


def rows_dot(rows, weight):
    return lax.dot_general(
        rows, weight, (((1,), (1,)), ((), ())), preferred_element_type=jnp.float32
    )


def silu(v):
    return v / (1.0 + jnp.exp(-v))


def mlp_kernel(rows, mine, x_ref, w_ref, out_ref, acc):
    step, last = pl.program_id(0), pl.num_programs(0) - 1
    parts = x_ref.shape[0]
    units = w_ref.shape[1] // 3
    x = jnp.concatenate([x_ref[t, :rows] for t in range(parts)], axis=1)

    def wide(first):
        return jnp.concatenate([w_ref[t, first : first + units] for t in range(parts)], axis=1)

    gate = rows_dot(x, wide(0))
    hidden = (silu(gate) * rows_dot(x, wide(units))).astype(jnp.bfloat16)
    for t in range(parts):
        term = jnp.dot(hidden, w_ref[t, 2 * units :], preferred_element_type=jnp.float32)

        @pl.when(step == 0)
        def _():
            acc[t] = term

        @pl.when(step > 0)
        def _():
            acc[t] += term

    @pl.when(step == last)
    def _():
        sums = sum(x_ref[t, rows:].astype(jnp.float32) for t in range(parts))
        shared = (silu(sums[: 2 * mine]) * sums[2 * mine :]).astype(jnp.bfloat16)
        for t in range(parts):
            out_ref[t, :rows] = acc[t].astype(jnp.bfloat16)
            out_ref[t, rows:] = shared


def expert_mlp(x, weights, rows, mine):
    parts, tall, width = x.shape
    units = weights.shape[1] // 3
    groups = weights.shape[0] // parts
    return pl.pallas_call(
        functools.partial(mlp_kernel, rows, mine),
        grid=(groups,),
        in_specs=[
            pl.BlockSpec((parts, tall, width), lambda i: (0, 0, 0)),
            pl.BlockSpec((parts, 3 * units, width), lambda i: (i, 0, 0)),
        ],
        out_specs=pl.BlockSpec((parts, rows + 2 * mine, width), lambda i: (0, 0, 0)),
        out_shape=jax.ShapeDtypeStruct((parts, rows + 2 * mine, width), jnp.bfloat16),
        scratch_shapes=[pltpu.VMEM((parts, rows, width), jnp.float32)],
        cost_estimate=pl.CostEstimate(
            flops=6 * groups * parts * rows * units * width,
            bytes_accessed=2 * (2 * x.size + weights.size),
            transcendentals=groups * rows * units,
        ),
        name="expert_mlp",
    )(x, weights)


def layer(
    tokens,
    routes,
    routing_weight,
    norm_gain_vector,
    expert_gate,
    expert_up,
    expert_down,
    shared_gate,
    shared_up,
    shared_down,
):
    tok_rows, width = tokens.shape
    groups, places, parts = (lax.axis_size(a) for a in ("grp", "fs", "tp"))
    model_width = width * parts
    experts, unit_rows, _ = expert_gate.shape
    top_count = routes.shape[1]
    capacity = tok_rows * top_count * 7 // (6 * experts)
    own = unit_rows // groups
    first = lax.axis_index("grp") * own

    gain = norm_gain_vector[None, None, :]

    def share(w):
        return lax.dynamic_slice_in_dim(w, first, own, axis=w.ndim - 2)

    def spread(w):
        return jnp.broadcast_to(share(w)[None], (experts, own, width))

    pieces = [
        (share(expert_gate) * gain).astype(jnp.bfloat16),
        (share(expert_up) * gain).astype(jnp.bfloat16),
        share(expert_down).astype(jnp.bfloat16),
        (spread(shared_gate) * gain).astype(jnp.bfloat16),
        (spread(shared_up) * gain).astype(jnp.bfloat16),
        spread(shared_down).astype(jnp.bfloat16),
    ]
    got = lax.all_to_all(
        jnp.concatenate(pieces, axis=1), "fs", split_axis=0, concat_axis=0, tiled=True
    )
    units = places * own
    got = got.reshape(places, 6, own, width).transpose(1, 0, 2, 3)
    whole = lax.all_gather(got[:3].reshape(3 * units, width), ("grp", "tp"), axis=0, tiled=False)
    served = lax.all_gather(got.reshape(6 * units, width), "grp", axis=0, tiled=False)

    values = tokens.astype(jnp.float32)
    totals = lax.psum(jnp.sum(values * values, axis=1), "tp")
    normed = (values * lax.rsqrt(totals / model_width + norm_eps)[:, None]).astype(jnp.bfloat16)
    named = routes.T[:, None, :] == jnp.arange(experts, dtype=jnp.int32)[None, :, None]
    member = jnp.any(named, axis=0)
    weight = jnp.sum(jnp.where(named, routing_weight.T[:, None, :], 0.0), axis=0)
    spot = jnp.arange(tok_rows, dtype=jnp.int32)
    before = (spot[:, None] < spot[None, :]).astype(jnp.bfloat16)
    slot = jnp.dot(
        member.astype(jnp.bfloat16), before, preferred_element_type=jnp.float32
    ).astype(jnp.int32)
    slot = jnp.where(member, slot, -1)
    placed = slot[:, None, :] == jnp.arange(capacity, dtype=jnp.int32)[None, :, None]
    placing = placed.astype(jnp.bfloat16).reshape(experts * capacity, tok_rows)
    high = lax.reduce_precision(weight, 8, 7)
    low = weight - high

    def weighted(w):
        return jnp.where(placed, w[:, None, :], 0.0).astype(jnp.bfloat16).reshape(
            experts * capacity, tok_rows
        )

    outgoing = jnp.dot(placing, normed, preferred_element_type=jnp.float32)
    outgoing = outgoing.astype(jnp.bfloat16).reshape(experts, capacity, width)
    incoming = lax.all_to_all(outgoing, "fs", split_axis=0, concat_axis=0, tiled=True)
    incoming, served = lax.optimization_barrier((incoming, served))
    served = served.reshape(groups, 6, places, own, width).transpose(1, 2, 0, 3, 4)
    served = served.reshape(6, groups * units, width)
    gate_new, up_new, down_new, shared_g, shared_u, shared_d = (served[i] for i in range(6))
    rows, mine = places * capacity // parts, tok_rows // parts
    slabs = [
        half.reshape(parts, mine, width)
        for w in (shared_g, shared_u)
        for half in jnp.split(rows_dot(normed, w).astype(jnp.bfloat16), w.shape[0] // width, 1)
    ]
    gathered = lax.all_to_all(
        jnp.concatenate([incoming.reshape(parts, rows, width)] + slabs, axis=1),
        "tp",
        split_axis=0,
        concat_axis=0,
        tiled=True,
    )
    produced = expert_mlp(gathered, whole, rows, mine)
    produced = lax.all_to_all(produced, "tp", split_axis=0, concat_axis=0, tiled=True)
    shared_hidden = produced[:, rows:].reshape(parts, -1, mine, width).transpose(0, 2, 1, 3)
    shared_hidden = shared_hidden.reshape(tok_rows, -1)
    shared_out = jnp.dot(shared_hidden, shared_d, preferred_element_type=jnp.float32)
    heavy, light = weighted(high), weighted(low)
    produced, shared_out, heavy, light, gate_new, up_new, down_new, shared_g, shared_u, shared_d = (
        lax.optimization_barrier(
            (
                produced[:, :rows].reshape(places, capacity, width),
                shared_out,
                heavy,
                light,
                gate_new,
                up_new,
                down_new,
                shared_g,
                shared_u,
                shared_d,
            )
        )
    )
    returned = lax.all_to_all(produced, "fs", split_axis=0, concat_axis=0, tiled=True)
    returned = returned.reshape(experts * capacity, width)

    def taken(w):
        return lax.dot_general(
            w, returned, (((0,), (0,)), ((), ())), preferred_element_type=jnp.float32
        )

    mixed = (taken(heavy) + taken(light) + shared_out).astype(jnp.bfloat16)
    return (
        mixed,
        gate_new[None],
        up_new[None],
        down_new[None],
        shared_g,
        shared_u,
        shared_d,
    )


def solution(mesh):
    return jax.shard_map(
        layer,
        mesh=mesh,
        in_specs=(
            P(("grp", "fs"), "tp"),
            P(("grp", "fs"), None),
            P(("grp", "fs"), None),
            P("tp"),
            P(None, "fs", "tp"),
            P(None, "fs", "tp"),
            P(None, "fs", "tp"),
            P("fs", "tp"),
            P("fs", "tp"),
            P("fs", "tp"),
        ),
        out_specs=(
            P(("grp", "fs"), "tp"),
            P(("grp", "fs"), None, "tp"),
            P(("grp", "fs"), None, "tp"),
            P(("grp", "fs"), None, "tp"),
            P("grp", "tp"),
            P("grp", "tp"),
            P("grp", "tp"),
        ),
        check_vma=False,
    )
```

time: 472 us -> 436 us (0.924)
  waiting for transfers between devices: 105 us -> 12 us
  blocking collectives: 316 us -> 377 us
    all_to_all x2, blocking collectives: 40.4 us -> 131 us  [the longest x1 107 us: layer(): lax.all_to_all(produced, 'fs', split_axis=0, concat_axis=0, tiled=True)]
    reduce_scatter x1 -> x0, waiting for transfers between devices: 44 us -> none  [layer(): lax.psum_scatter(partial.reshape(tok_rows, parts, 2 * share_units).transp...]
    all_gather x2, waiting for transfers between devices: 29.2 us -> 0.01 us  [the longest x1 0.01 us: layer(): lax.all_gather(got.reshape(6 * units, width), 'grp', axis=0, tiled=False)]
    all_to_all x1, waiting for transfers between devices: 31.5 us -> 11.9 us  [layer(): lax.all_to_all(produced, 'tp', split_axis=0, concat_axis=0, tiled=True)]
    all_to_all x1, blocking collectives: 117 us -> 99.7 us  [layer(): lax.all_to_all(outgoing, 'fs', split_axis=0, concat_axis=0, tiled=True)]
    all_gather x1 -> x0, blocking collectives: 13.9 us -> none  [layer(): shared_hidden = lax.all_gather(shared_hidden, 'tp', axis=1, tiled=True)]
  transfers between devices with their start and end apart: 4 -> 3, of which waited for: 3 -> 1; matrix products, arithmetic and copies ran while one was open for 1% -> 2% of each run, Pallas kernels for 0% -> 0%
where the time goes in v2:
time: 436 us; the launch traced here: 435 us
  blocking collectives  377 us (86%)
  between operations  14.3 us (3%)
  waiting for transfers between devices  12 us (3%)
  local copies, waits for them, and re-layouts  10.9 us (2%)
  Pallas kernels  8.38 us (2%)
  starting transfers between devices  4.78 us (1%)
    all_to_all x1, blocking collectives, layer(): lax.all_to_all(jnp.concatenate(pieces, axis=1), 'fs', split_axis=0, conca...  132 us
    all_to_all x1, blocking collectives, layer(): lax.all_to_all(produced, 'fs', split_axis=0, concat_axis=0, tiled=True)  107 us
    all_to_all x1, blocking collectives, layer(): lax.all_to_all(outgoing, 'fs', split_axis=0, concat_axis=0, tiled=True)  99.7 us
    all_to_all x1, blocking collectives, layer(): lax.all_to_all(jnp.concatenate([incoming.reshape(parts, rows, width)] + s...  24.4 us
    psum x1, blocking collectives, layer(): totals = lax.psum(jnp.sum(values * values, axis=1), 'tp')  13.4 us
    all_to_all x1, waiting for transfers between devices, layer(): lax.all_to_all(produced, 'tp', split_axis=0, concat_axis=0, tiled=True)  11.9 us
  transfers between devices with their start and end apart: 3, of which 1 were waited for; matrix products, arithmetic and copies ran while one was open for 2% of the time, Pallas kernels for 0%

profile of v2, /device:TPU:33, one launch (start us, length us, event | category | flops | bytes accessed | tf_op | source)
XLA Modules:
  0.0 434.9 jit_solution(12409454696960237612)
XLA Ops:
  7.2 0.0 copy-start
  7.2 0.1 all-gather.3.cloned.1.call-start
  7.3 0.6 copy-done
  7.9 1.0 fusion.8
  8.9 1.0 fusion.9
  9.9 1.0 fusion.10
  10.8 0.7 constant_dynamic-slice_fusion
  11.6 0.7 fusion.11
  12.3 0.7 fusion.12
  13.0 132.0 %all_to_all.25 = bf16[32,48,256]{2,1,0:T(8,128)(2,1)S(1)} all-to-all(bf16[32,48,256]{2,1,0:T(8,128)(2,1)S(1)} %broadcast_dynamic-update-slice_fusion), channel_id=1, replica_groups=mesh['grp'=2,'fs'=32,'tp'=8] {'fs'}, dimensions={0} | all-to-all | bytes 1572864 | tf_op jit(solution)/shard_map/all_to_all | solution.py:114
  145.0 1.1 copy_bitcast_fusion
  146.1 0.0 copy-start.6
  146.1 0.0 copy-start.1
  146.1 0.1 all-gather.3.cloned.1.call-update
  146.2 0.1 all-gather.5.cloned.1.call-start
  146.3 0.8 slice.44
  147.1 0.1 all-gather.5.cloned.1.call-update
  147.2 0.1 eq.41
  147.2 0.0 copy-done.6
  147.3 0.1 fusion.4
  147.4 0.3 bitcast_compare_fusion
  147.8 0.0 copy-done.1
  147.8 0.1 fusion.6
  147.9 13.4 %psum.7 = f32[192]{0:T(256)S(1)} all-reduce(f32[192]{0:T(256)S(1)} %fusion.6), channel_id=1, replica_groups=mesh['grp'=2,'fs'=32,'tp'=8] {'tp'}, use_global_device_ids=true, to_apply=%region_2.0 | all-reduce | flops 192 | bytes 1536 | tf_op jit(solution)/shard_map/psum | solution.py:123
  161.4 0.5 convolution_convert_fusion
  161.8 99.7 %all_to_all.26 = bf16[32,56,256]{2,1,0:T(8,128)(2,1)S(1)} all-to-all(bf16[32,56,256]{2,1,0:T(8,128)(2,1)S(1)} %bitcast.65), channel_id=1, replica_groups=mesh['grp'=2,'fs'=32,'tp'=8] {'fs'}, dimensions={0} | all-to-all | bytes 1835008 | tf_op jit(solution)/shard_map/all_to_all | solution.py:146
  261.5 0.0 all-gather.3.cloned.1.call-done
  261.5 2.2 fusion.16
  263.8 0.0 copy-start.4
  263.8 0.0 copy-start.5
  263.8 0.1 bitcast_dynamic-update-slice_fusion
  263.9 0.2 convolution_convert_fusion.2
  264.1 0.3 copy-done.4
  264.5 0.0 copy-done.5
  264.6 0.2 convolution_convert_fusion.1
  264.9 24.4 %all_to_all.27.x_ref = bf16[8,320,256]{2,1,0:T(8,128)(2,1)} all-to-all(bf16[8,320,256]{2,1,0:T(8,128)(2,1)S(1)} %constant_dynamic-update-slice_fusion), channel_id=1, replica_groups=mesh['grp'=2,'fs'=32,'tp'=8] {'tp'}, dimensions={0} | all-to-all | bytes 2621440 | tf_op jit(solution)/shard_map/all_to_all | solution.py:157
  289.3 0.0 all-gather.5.cloned.1.call-done.w_ref
  289.3 8.4 %expert_mlp.1 = bf16[8,272,256]{2,1,0:T(8,128)(2,1)} custom-call(bf16[8,320,256]{2,1,0:T(8,128)(2,1)} %all_to_all.27.x_ref, bf16[16,768,256]{2,1,0:T(8,128)(2,1)} %all-gather.5.cloned.1.call-done.w_ref), custom_call_target="tpu_custom_call" | custom-call | flops 1409286144 | bytes 8912896 | tf_op jit(solution)/shard_map/expert_mlp/pallas_call | solution.py:58
  297.7 0.0 copy-start.7
  297.7 4.7 %all-to-all-start.3 = ((bf16[8,272,256]{2,1,0:T(8,128)(2,1)}), bf16[8,272,256]{2,1,0:T(8,128)(2,1)S(1)}, u32[]{:S(2)}, u32[]{:S(2)}) async-start(bf16[8,272,256]{2,1,0:T(8,128)(2,1)} %expert_mlp.1), calls=%async_computation.3 | async-start | bytes 2228224 | tf_op jit(solution)/shard_map/all_to_all | solution.py:165
  302.3 0.0 copy-start.3
  302.3 0.0 copy-start.2
  302.3 0.0 copy-done.7
  302.4 0.3 fusion
  302.7 0.6 copy-done.3
  303.3 0.7 copy.40
  304.0 0.0 copy-done.2
  304.0 0.7 copy.41
  304.7 0.7 copy.42
  305.4 0.7 copy.43
  306.2 11.9 %all-to-all-done.3 = bf16[8,272,256]{2,1,0:T(8,128)(2,1)S(1)} async-done(((bf16[8,272,256]{2,1,0:T(8,128)(2,1)}), bf16[8,272,256]{2,1,0:T(8,128)(2,1)S(1)}, u32[]{:S(2)}, u32[]{:S(2)}) %all-to-all-start.3) | async-done | bytes 1114144 | tf_op jit(solution)/shard_map/all_to_all | solution.py:165
  318.1 0.2 copy.39
  318.3 1.2 fusion.19
  319.5 0.1 slice.45
  319.5 106.9 %all_to_all.28 = bf16[32,56,256]{2,1,0:T(8,128)(2,1)S(1)} all-to-all(bf16[32,56,256]{2,1,0:T(8,128)(2,1)S(1)} %bitcast.64), channel_id=1, replica_groups=mesh['grp'=2,'fs'=32,'tp'=8] {'fs'}, dimensions={0} | all-to-all | bytes 1835008 | tf_op jit(solution)/shard_map/all_to_all | solution.py:186
  426.5 0.5 fusion.20
  427.0 1.1 fusion.3
  (17 shorter events, 0.2 us)
Async XLA Ops:
  7.2 0.7 copy-start
  7.2 254.3 %all-gather.3.cloned.1.call-start = ((), (), s32[]{:S(2)}) async-start(), calls=%async_computation.5 | async-start | bytes 2359296 | tf_op jit(solution)/shard_map/all_gather | solution.py:120
  146.1 1.1 copy-start.6
  146.1 1.6 copy-start.1
  146.2 143.1 %all-gather.5.cloned.1.call-start = ((), (), s32[]{:S(2)}) async-start(), calls=%async_computation.6 | async-start | bytes 6684672 | tf_op jit(solution)/shard_map/all_gather | solution.py:119
  263.8 0.7 copy-start.4
  263.8 0.8 copy-start.5
  297.7 4.7 %copy-start.7 = (f32[192,8]{0,1:T(8,128)S(1)}, f32[192,8]{0,1:T(8,128)}, u32[]{:S(2)}) copy-start(f32[192,8]{0,1:T(8,128)} %param.12) | copy-start | bytes 18436
  297.7 20.4 %all-to-all-start.3 = ((bf16[8,272,256]{2,1,0:T(8,128)(2,1)}), bf16[8,272,256]{2,1,0:T(8,128)(2,1)S(1)}, u32[]{:S(2)}, u32[]{:S(2)}) async-start(bf16[8,272,256]{2,1,0:T(8,128)(2,1)} %expert_mlp.1), calls=%async_computation.3 | async-start | bytes 2228224 | tf_op jit(solution)/shard_map/all_to_all | solution.py:165
  302.3 0.9 copy-start.3
  302.3 1.7 copy-start.2
Sparse Core Ops, SparseCore 0:
  146.3 29.1 all-gather.2
  178.9 95.5 all-gather.4

commit v3 on v1

v3 whole, which is shorter than its diff:
```python
import jax
import jax.numpy as jnp
from jax import lax
from jax.experimental import pallas as pl
from jax.experimental.pallas import tpu as pltpu
from jax.sharding import Mesh
from jax.sharding import PartitionSpec as P

norm_eps = 1e-06


def rows_dot(rows, weight):
    return lax.dot_general(
        rows, weight, (((1,), (1,)), ((), ())), preferred_element_type=jnp.float32
    )


def silu(v):
    return v / (1.0 + jnp.exp(-v))


def mlp_kernel(x_ref, w_ref, out_ref, acc):
    step, last = pl.program_id(0), pl.num_programs(0) - 1
    parts = x_ref.shape[0]
    units = w_ref.shape[1] // 3
    x = jnp.concatenate([x_ref[t] for t in range(parts)], axis=1)

    def wide(first):
        return jnp.concatenate([w_ref[t, first : first + units] for t in range(parts)], axis=1)

    gate = rows_dot(x, wide(0))
    hidden = (silu(gate) * rows_dot(x, wide(units))).astype(jnp.bfloat16)
    for t in range(parts):
        term = jnp.dot(hidden, w_ref[t, 2 * units :], preferred_element_type=jnp.float32)

        @pl.when(step == 0)
        def _():
            acc[t] = term

        @pl.when(step > 0)
        def _():
            acc[t] += term

    @pl.when(step == last)
    def _():
        out_ref[...] = acc[...].astype(jnp.bfloat16)


def expert_mlp(x, weights):
    parts, rows, width = x.shape
    units = weights.shape[1] // 3
    groups = weights.shape[0] // parts
    return pl.pallas_call(
        mlp_kernel,
        grid=(groups,),
        in_specs=[
            pl.BlockSpec((parts, rows, width), lambda i: (0, 0, 0)),
            pl.BlockSpec((parts, 3 * units, width), lambda i: (i, 0, 0)),
        ],
        out_specs=pl.BlockSpec((parts, rows, width), lambda i: (0, 0, 0)),
        out_shape=jax.ShapeDtypeStruct((parts, rows, width), jnp.bfloat16),
        scratch_shapes=[pltpu.VMEM((parts, rows, width), jnp.float32)],
        cost_estimate=pl.CostEstimate(
            flops=6 * groups * parts * rows * units * width,
            bytes_accessed=2 * (2 * x.size + weights.size),
            transcendentals=groups * rows * units,
        ),
        name="expert_mlp",
    )(x, weights)


fs = ("fh", "fl")


def layer(
    tokens,
    routes,
    routing_weight,
    norm_gain_vector,
    expert_gate,
    expert_up,
    expert_down,
    shared_gate,
    shared_up,
    shared_down,
):
    tok_rows, width = tokens.shape
    groups, places, parts = lax.axis_size("grp"), lax.axis_size(fs), lax.axis_size("tp")
    model_width = width * parts
    experts, unit_rows, _ = expert_gate.shape
    top_count = routes.shape[1]
    capacity = tok_rows * top_count * 7 // (6 * experts)
    own = unit_rows // groups
    first = lax.axis_index("grp") * own

    gain = norm_gain_vector[None, None, :]

    def share(w):
        return lax.dynamic_slice_in_dim(w, first, own, axis=w.ndim - 2)

    pieces = [
        (share(expert_gate) * gain).astype(jnp.bfloat16),
        (share(expert_up) * gain).astype(jnp.bfloat16),
        share(expert_down).astype(jnp.bfloat16),
    ]
    got = lax.all_to_all(
        jnp.concatenate(pieces, axis=1), fs, split_axis=0, concat_axis=0, tiled=True
    )
    units = places * own
    got = got.reshape(places, 3, own, width).transpose(1, 0, 2, 3).reshape(3 * units, width)
    whole = lax.all_gather(got, ("grp", "tp"), axis=0, tiled=False)
    served = lax.all_gather(got, "grp", axis=0, tiled=False)
    served = served.reshape(groups, 3, places, own, width).transpose(1, 2, 0, 3, 4)
    served = served.reshape(3, 1, groups * units, width)
    gate_new, up_new, down_new = served[0], served[1], served[2]

    block = jnp.concatenate(
        [
            (shared_gate * gain[0]).astype(jnp.bfloat16),
            (shared_up * gain[0]).astype(jnp.bfloat16),
            shared_down.astype(jnp.bfloat16),
        ],
        axis=1,
    )
    block = lax.all_gather(block, "fh", axis=0, tiled=True)
    block = jnp.pad(block, ((0, 0), (0, width)))
    block = lax.all_gather(block, "fl", axis=0, tiled=True)
    block = block.reshape(lax.axis_size("fl"), lax.axis_size("fh"), unit_rows, 4 * width)
    block = block.transpose(1, 0, 2, 3).reshape(places * unit_rows, 4 * width)
    shared_g, shared_u, shared_d = (block[:, i * width : (i + 1) * width] for i in range(3))
    units = places * unit_rows

    values = tokens.astype(jnp.float32)
    totals = lax.psum(jnp.sum(values * values, axis=1), "tp")
    normed = (values * lax.rsqrt(totals / model_width + norm_eps)[:, None]).astype(jnp.bfloat16)
    named = routes.T[:, None, :] == jnp.arange(experts, dtype=jnp.int32)[None, :, None]
    member = jnp.any(named, axis=0)
    weight = jnp.sum(jnp.where(named, routing_weight.T[:, None, :], 0.0), axis=0)
    spot = jnp.arange(tok_rows, dtype=jnp.int32)
    before = (spot[:, None] < spot[None, :]).astype(jnp.bfloat16)
    slot = jnp.dot(
        member.astype(jnp.bfloat16), before, preferred_element_type=jnp.float32
    ).astype(jnp.int32)
    slot = jnp.where(member, slot, -1)
    placed = slot[:, None, :] == jnp.arange(capacity, dtype=jnp.int32)[None, :, None]
    placing = placed.astype(jnp.bfloat16).reshape(experts * capacity, tok_rows)
    high = lax.reduce_precision(weight, 8, 7)
    low = weight - high

    def weighted(w):
        return jnp.where(placed, w[:, None, :], 0.0).astype(jnp.bfloat16).reshape(
            experts * capacity, tok_rows
        )

    outgoing = jnp.dot(placing, normed, preferred_element_type=jnp.float32)
    outgoing = outgoing.astype(jnp.bfloat16).reshape(experts, capacity, width)
    incoming = lax.all_to_all(outgoing, fs, split_axis=0, concat_axis=0, tiled=True)
    chunk = places * capacity // parts
    gathered = lax.all_to_all(
        incoming.reshape(parts, chunk, width), "tp", split_axis=0, concat_axis=0, tiled=True
    )
    produced = expert_mlp(gathered, whole)
    produced = lax.all_to_all(produced, "tp", split_axis=0, concat_axis=0, tiled=True)
    returned = lax.all_to_all(
        produced.reshape(places, capacity, width), fs, split_axis=0, concat_axis=0, tiled=True
    )
    returned = returned.reshape(experts * capacity, width)

    share_units = units // parts
    both = jnp.concatenate(
        [shared_g.reshape(parts, share_units, width), shared_u.reshape(parts, share_units, width)],
        axis=1,
    ).reshape(2 * units, width)
    partial = rows_dot(normed, both).astype(jnp.bfloat16)
    sums = lax.psum_scatter(
        partial.reshape(tok_rows, parts, 2 * share_units).transpose(1, 0, 2),
        "tp",
        scatter_dimension=0,
        tiled=False,
    ).astype(jnp.float32)
    shared_hidden = (jax.nn.silu(sums[:, :share_units]) * sums[:, share_units:]).astype(
        jnp.bfloat16
    )
    shared_hidden = lax.all_gather(shared_hidden, "tp", axis=1, tiled=True)
    shared_out = jnp.dot(shared_hidden, shared_d, preferred_element_type=jnp.float32)

    def taken(w):
        return lax.dot_general(
            weighted(w), returned, (((0,), (0,)), ((), ())), preferred_element_type=jnp.float32
        )

    mixed = (taken(high) + taken(low) + shared_out).astype(jnp.bfloat16)
    return (
        mixed,
        gate_new,
        up_new,
        down_new,
        shared_g,
        shared_u,
        shared_d,
    )


def solution(mesh):
    count = mesh.shape["fs"]
    low = 8 if count % 8 == 0 else 1
    cut = Mesh(
        mesh.devices.reshape(mesh.shape["grp"], count // low, low, mesh.shape["tp"]),
        ("grp",) + fs + ("tp",),
    )
    line = ("grp",) + fs
    return jax.shard_map(
        layer,
        mesh=cut,
        in_specs=(
            P(line, "tp"),
            P(line, None),
            P(line, None),
            P("tp"),
            P(None, fs, "tp"),
            P(None, fs, "tp"),
            P(None, fs, "tp"),
            P(fs, "tp"),
            P(fs, "tp"),
            P(fs, "tp"),
        ),
        out_specs=(
            P(line, "tp"),
            P(line, None, "tp"),
            P(line, None, "tp"),
            P(line, None, "tp"),
            P("grp", "tp"),
            P("grp", "tp"),
            P("grp", "tp"),
        ),
        check_vma=False,
    )
```

time: 472 us -> 529 us (1.12)
  blocking collectives: 316 us -> 379 us
    all_gather x0 -> x2, blocking collectives: none -> 114 us  [the longest x1 103 us: layer(): block = lax.all_gather(block, 'fh', axis=0, tiled=True)]
    all_to_all x2, blocking collectives: 249 us -> 196 us  [the longest x1 98.9 us: layer(): lax.all_to_all(outgoing, fs, split_axis=0, concat_axis=0, tiled=True)]
    all_to_all x1, waiting for transfers between devices: 31.5 us -> 0.01 us  [layer(): lax.all_to_all(produced.reshape(places, capacity, width), fs, split_axis=...]
    all_gather x2, waiting for transfers between devices: 29.2 us -> 60.7 us  [the longest x1 60.7 us: layer(): block = lax.all_gather(block, 'fl', axis=0, tiled=True)]
  transfers between devices with their start and end apart: 4 -> 4, of which waited for: 3 -> 2; matrix products, arithmetic and copies ran while one was open for 1% -> 1% of each run, Pallas kernels for 0% -> 0%
where the time goes in v3:
time: 529 us
  blocking collectives  379 us (72%)
  waiting for transfers between devices  108 us (20%)
  between operations  15.9 us (3%)
  Pallas kernels  8.05 us (2%)
  local copies, waits for them, and re-layouts  7.88 us (1%)
    all_gather x1, blocking collectives, layer(): block = lax.all_gather(block, 'fh', axis=0, tiled=True)  103 us
    all_to_all x1, blocking collectives, layer(): lax.all_to_all(outgoing, fs, split_axis=0, concat_axis=0, tiled=True)  98.9 us
    all_to_all x1, blocking collectives, layer(): lax.all_to_all(jnp.concatenate(pieces, axis=1), fs, split_axis=0, concat_...  97.4 us
    all_gather x1, waiting for transfers between devices, layer(): block = lax.all_gather(block, 'fl', axis=0, tiled=True)  60.7 us
    reduce_scatter x1, waiting for transfers between devices, layer(): lax.psum_scatter(partial.reshape(tok_rows, parts, 2 * share_units).transp...  47.5 us
    all_to_all x1, blocking collectives, layer(): lax.all_to_all(incoming.reshape(parts, chunk, width), 'tp', split_axis=0,...  21.1 us
    all_to_all x1, blocking collectives, layer(): lax.all_to_all(produced, 'tp', split_axis=0, concat_axis=0, tiled=True)  19 us
    psum x1, blocking collectives, layer(): totals = lax.psum(jnp.sum(values * values, axis=1), 'tp')  14.9 us
  transfers between devices with their start and end apart: 4, of which 2 were waited for; matrix products, arithmetic and copies ran while one was open for 1% of the time, Pallas kernels for 0%

profile of v3, /device:TPU:33, one launch (start us, length us, event | category | flops | bytes accessed | tf_op | source)
XLA Modules:
  0.0 528.5 jit_solution(15096581404570301814)
XLA Ops:
  8.0 0.0 copy-start
  8.1 0.1 all-gather.3.cloned.1.call-start
  8.1 1.0 copy-done
  9.1 0.0 copy-start.6
  9.1 1.1 multiply_convert_fusion.1
  10.2 0.0 copy-start.5
  10.3 97.4 %all_to_all.25 = bf16[32,24,256]{2,1,0:T(8,128)(2,1)S(1)} all-to-all(bf16[32,24,256]{2,1,0:T(8,128)(2,1)S(1)} %pad_maximum_fusion.1), channel_id=1, replica_groups=mesh['grp'=2,'fh'=4,'fl'=8,'tp'=8] {'fh','fl'}, dimensions={0} | all-to-all | bytes 786432 | tf_op jit(solution)/shard_map/all_to_all | solution.py:106
  107.7 0.8 copy.36
  108.5 0.1 all-gather.3.cloned.1.call-update
  108.5 0.1 eq.45
  108.6 0.0 copy-done.6
  108.7 0.1 fusion.3
  108.8 0.3 bitcast_compare_fusion
  109.1 0.0 copy-done.5
  109.2 0.1 fusion.11
  109.3 14.9 %psum.7 = f32[192]{0:T(256)S(1)} all-reduce(f32[192]{0:T(256)S(1)} %fusion.11), channel_id=1, replica_groups=mesh['grp'=2,'fh'=4,'fl'=8,'tp'=8] {'tp'}, use_global_device_ids=true, to_apply=%region_3.4 | all-reduce | flops 192 | bytes 1536 | tf_op jit(solution)/shard_map/psum | solution.py:134
  124.2 0.5 convolution_convert_fusion
  124.7 98.9 %all_to_all.26 = bf16[32,56,256]{2,1,0:T(8,128)(2,1)S(1)} all-to-all(bf16[32,56,256]{2,1,0:T(8,128)(2,1)S(1)} %bitcast.48), channel_id=1, replica_groups=mesh['grp'=2,'fh'=4,'fl'=8,'tp'=8] {'fh','fl'}, dimensions={0} | all-to-all | bytes 1835008 | tf_op jit(solution)/shard_map/all_to_all | solution.py:157
  223.5 21.1 %all_to_all.27.x_ref = bf16[8,224,256]{2,1,0:T(8,128)(2,1)} all-to-all(bf16[8,224,256]{2,1,0:T(8,128)(2,1)S(1)} %bitcast.49), channel_id=1, replica_groups=mesh['grp'=2,'fh'=4,'fl'=8,'tp'=8] {'tp'}, dimensions={0} | all-to-all | bytes 1835008 | tf_op jit(solution)/shard_map/all_to_all | solution.py:159
  244.6 0.0 all-gather.3.cloned.1.call-done.w_ref
  244.6 8.0 %expert_mlp.1 = bf16[8,224,256]{2,1,0:T(8,128)(2,1)} custom-call(bf16[8,224,256]{2,1,0:T(8,128)(2,1)} %all_to_all.27.x_ref, bf16[16,768,256]{2,1,0:T(8,128)(2,1)} %all-gather.3.cloned.1.call-done.w_ref), custom_call_target="tpu_custom_call" | custom-call | flops 1409286144 | bytes 8126464 | tf_op jit(solution)/shard_map/expert_mlp/pallas_call | solution.py:53
  252.6 0.0 copy-start.9
  252.6 0.0 copy-start.7
  252.6 0.0 copy-start.8
  252.6 0.0 copy-start.11
  252.7 19.0 %all_to_all.28 = bf16[8,224,256]{2,1,0:T(8,128)(2,1)} all-to-all(bf16[8,224,256]{2,1,0:T(8,128)(2,1)} %expert_mlp.1), channel_id=1, replica_groups=mesh['grp'=2,'fh'=4,'fl'=8,'tp'=8] {'tp'}, dimensions={0} | all-to-all | bytes 1835008 | tf_op jit(solution)/shard_map/all_to_all | solution.py:163
  271.7 4.8 all-to-all-start.4
  276.5 0.1 all-gather.5.cloned.1.call-start
  276.6 0.0 copy-done.9
  276.6 0.0 copy-done.7
  276.6 0.0 copy-done.8
  276.6 0.0 copy-done.11
  276.7 102.6 %all_gather.16 = bf16[64,768]{1,0:T(8,128)(2,1)S(1)} all-gather(bf16[16,768]{1,0:T(8,128)(2,1)S(1)} %pad_maximum_fusion.2), channel_id=1, replica_groups=mesh['grp'=2,'fh'=4,'fl'=8,'tp'=8] {'fh'}, dimensions={0}, use_global_device_ids=true | all-gather | bytes 122880 | tf_op jit(solution)/shard_map/all_gather | solution.py:125
  379.2 0.7 pad.4
  379.9 0.1 all-gather.5.cloned.1.call-update
  380.0 0.1 reduce-scatter.2.cloned.1.call-start
  380.0 60.7 %all-gather.5.cloned.1.call-done = bf16[512,1024]{1,0:T(8,128)(2,1)} async-done(((bf16[64,1024]{1,0:T(8,128)(2,1)}), bf16[512,1024]{1,0:T(8,128)(2,1)}) %all-gather.5.cloned.1.call-update) | async-done | bytes 1048592 | tf_op jit(solution)/shard_map/all_gather | solution.py:127
  440.7 1.3 copy.37
  442.0 0.1 fusion.18
  442.1 0.0 copy-start.3
  442.1 0.0 copy-start.4
  442.1 0.0 copy-start.2
  442.1 0.0 copy-start.10
  442.1 0.0 copy-start.1
  442.2 0.3 fusion
  442.5 0.8 copy.45
  443.3 0.1 reduce-scatter.2.cloned.1.call-update
  443.4 0.0 copy-done.10
  443.5 47.5 %reduce-scatter.2.cloned.1.call-done = bf16[1,192,128]{2,1,0:T(8,128)(2,1)} async-done(((bf16[8,192,128]{2,1,0:T(8,128)(2,1)}), bf16[1,192,128]{2,1,0:T(8,128)(2,1)}) %reduce-scatter.2.cloned.1.call-update) | async-done | bytes 49168 | tf_op jit(solution)/shard_map/reduce_scatter | solution.py:175
  491.0 0.9 copy.39
  491.9 0.0 copy-done.3
  491.9 0.0 copy-done.4
  492.0 13.8 %all_gather.18 = bf16[192,512]{0,1:T(8,128)(2,1)S(1)} all-gather(bf16[192,64]{0,1:T(8,128)(2,1)S(1)} %fusion.13), channel_id=1, replica_groups=mesh['grp'=2,'fh'=4,'fl'=8,'tp'=8] {'tp'}, dimensions={1}, use_global_device_ids=true | all-gather | bytes 221184 | tf_op jit(solution)/shard_map/all_gather | solution.py:184
  505.8 0.0 copy-done.1
  505.8 11.2 %all_gather.19 = bf16[2,768,256]{2,1,0:T(8,128)(2,1)S(1)} all-gather(bf16[1,768,256]{2,1,0:T(8,128)(2,1)S(1)} %bitcast.51), channel_id=1, replica_groups=mesh['grp'=2,'fh'=4,'fl'=8,'tp'=8] {'grp'}, dimensions={0}, use_global_device_ids=true | all-gather | bytes 1179648 | tf_op jit(solution)/shard_map/all_gather | solution.py:112
  517.0 0.1 fusion.19
  517.0 0.7 copy.40
  517.8 0.7 copy.41
  518.5 0.7 copy.42
  519.2 0.0 all-to-all-done.4
  519.2 0.5 convolution_bitcast_fusion
  519.7 0.5 fusion.1
  520.2 0.0 copy-done.2
  520.2 0.9 fusion.2
  (13 shorter events, 0.2 us)
Async XLA Ops:
  8.0 1.0 copy-start
  8.1 236.5 %all-gather.3.cloned.1.call-start = ((), (), s32[]{:S(2)}) async-start(), calls=%async_computation.6 | async-start | bytes 6684672 | tf_op jit(solution)/shard_map/all_gather | solution.py:111
  9.1 99.5 %copy-start.6 = (s32[192,8]{0,1:T(8,128)S(1)}, s32[192,8]{0,1:T(8,128)}, u32[]{:S(2)}) copy-start(s32[192,8]{0,1:T(8,128)} %param.11) | copy-start | bytes 18436
  10.2 98.9 %copy-start.5 = (bf16[192,256]{1,0:T(8,128)(2,1)S(1)}, bf16[192,256]{1,0:T(8,128)(2,1)}, u32[]{:S(2)}) copy-start(bf16[192,256]{1,0:T(8,128)(2,1)} %param.10) | copy-start | bytes 294916
  252.6 23.9 %copy-start.9 = (f32[16,256]{1,0:T(8,128)S(1)}, f32[16,256]{1,0:T(8,128)}, u32[]{:S(2)}) copy-start(f32[16,256]{1,0:T(8,128)} %param.19) | copy-start | bytes 49156
  252.6 24.0 %copy-start.7 = (f32[16,256]{1,0:T(8,128)S(1)}, f32[16,256]{1,0:T(8,128)}, u32[]{:S(2)}) copy-start(f32[16,256]{1,0:T(8,128)} %param.17) | copy-start | bytes 49156
  252.6 24.0 %copy-start.8 = (f32[16,256]{1,0:T(8,128)S(1)}, f32[16,256]{1,0:T(8,128)}, u32[]{:S(2)}) copy-start(f32[16,256]{1,0:T(8,128)} %param.18) | copy-start | bytes 49156
  252.6 24.0 %copy-start.11 = (f32[256]{0:T(256)S(1)}, f32[256]{0:T(256)}, u32[]{:S(2)}) copy-start(f32[256]{0:T(256)} %param.13) | copy-start | bytes 3076
  271.7 247.5 %all-to-all-start.4 = ((bf16[32,56,256]{2,1,0:T(8,128)(2,1)}), bf16[32,56,256]{2,1,0:T(8,128)(2,1)S(1)}, u32[]{:S(2)}, u32[]{:S(2)}) async-start(bf16[32,56,256]{2,1,0:T(8,128)(2,1)} %bitcast.8), calls=%async_computation.4 | async-start | bytes 1835008 | tf_op jit(solution)/shard_map/all_to_all | solution.py:164
  276.5 164.2 %all-gather.5.cloned.1.call-start = ((), (), s32[]{:S(2)}) async-start(), calls=%async_computation.7 | async-start | bytes 1179648 | tf_op jit(solution)/shard_map/all_gather | solution.py:127
  380.0 111.0 %reduce-scatter.2.cloned.1.call-start = ((), (), s32[]{:S(2)}) async-start(), calls=%async_computation.8 | async-start | bytes 442368 | tf_op jit(solution)/shard_map/reduce_scatter | solution.py:175
  442.1 49.8 %copy-start.3 = (bf16[512,256]{1,0:T(8,128)(2,1)}, bf16[512,256]{1,0:T(8,128)(2,1)S(1)}, u32[]{:S(2)}) copy-start(bf16[512,256]{1,0:T(8,128)(2,1)S(1)} %get-tuple-element.8) | copy-start | bytes 786436
  442.1 49.8 %copy-start.4 = (bf16[512,256]{1,0:T(8,128)(2,1)}, bf16[512,256]{1,0:T(8,128)(2,1)S(1)}, u32[]{:S(2)}) copy-start(bf16[512,256]{1,0:T(8,128)(2,1)S(1)} %get-tuple-element.9) | copy-start | bytes 786436
  442.1 78.1 %copy-start.2 = (bf16[512,256]{1,0:T(8,128)(2,1)}, bf16[512,256]{1,0:T(8,128)(2,1)S(1)}, u32[]{:S(2)}) copy-start(bf16[512,256]{1,0:T(8,128)(2,1)S(1)} %get-tuple-element.7) | copy-start | bytes 786436
  442.1 1.3 copy-start.10
  442.1 63.7 %copy-start.1 = (bf16[32,3,8,256]{3,2,0,1:T(8,128)(2,1)S(1)}, bf16[32,3,8,256]{3,2,0,1:T(8,128)(2,1)}, u32[]{:S(2)}) copy-start(bf16[32,3,8,256]{3,2,0,1:T(8,128)(2,1)} %copy.36) | copy-start | bytes 1179652
Sparse Core Ops, SparseCore 0:
  108.6 79.1 all-gather.2
Sparse Core Ops, SparseCore 1:
  380.0 60.6 all-gather.4
  443.5 47.4 reduce-scatter.1

commit v4 on v3

--- a/solution.py
+++ b/solution.py
@@ -19,54 +19,60 @@
     return v / (1.0 + jnp.exp(-v))
 
 
-def mlp_kernel(x_ref, w_ref, out_ref, acc):
+def mlp_kernel(x_ref, gate_ref, up_ref, down_ref, out_ref, acc):
     step, last = pl.program_id(0), pl.num_programs(0) - 1
     parts = x_ref.shape[0]
-    units = w_ref.shape[1] // 3
-    x = jnp.concatenate([x_ref[t] for t in range(parts)], axis=1)
-
-    def wide(first):
-        return jnp.concatenate([w_ref[t, first : first + units] for t in range(parts)], axis=1)
-
-    gate = rows_dot(x, wide(0))
-    hidden = (silu(gate) * rows_dot(x, wide(units))).astype(jnp.bfloat16)
+
+    def wide(ref):
+        return jnp.concatenate([ref[t] for t in range(parts)], axis=1)
+
+    x = wide(x_ref)
+    gate = rows_dot(x, wide(gate_ref))
+    hidden = (silu(gate) * rows_dot(x, wide(up_ref))).astype(jnp.bfloat16)
     for t in range(parts):
-        term = jnp.dot(hidden, w_ref[t, 2 * units :], preferred_element_type=jnp.float32)
+        term = jnp.dot(hidden, down_ref[t], preferred_element_type=jnp.float32)
 
         @pl.when(step == 0)
         def _():
             acc[t] = term
 
-        @pl.when(step > 0)
+        @pl.when((step > 0) & (step < last))
         def _():
             acc[t] += term
 
-    @pl.when(step == last)
-    def _():
-        out_ref[...] = acc[...].astype(jnp.bfloat16)
+        @pl.when((step > 0) & (step == last))
+        def _():
+            out_ref[t] = (acc[t] + term).astype(jnp.bfloat16)
 
 
 def expert_mlp(x, weights):
     parts, rows, width = x.shape
     units = weights.shape[1] // 3
-    groups = weights.shape[0] // parts
+    chunk = units // 2
+    steps = units // chunk
+
+    def part(first):
+        return pl.BlockSpec((parts, chunk, width), lambda i: (0, first * steps + i, 0))
+
     return pl.pallas_call(
         mlp_kernel,
-        grid=(groups,),
+        grid=(steps,),
         in_specs=[
             pl.BlockSpec((parts, rows, width), lambda i: (0, 0, 0)),
-            pl.BlockSpec((parts, 3 * units, width), lambda i: (i, 0, 0)),
+            part(0),
+            part(1),
+            part(2),
         ],
         out_specs=pl.BlockSpec((parts, rows, width), lambda i: (0, 0, 0)),
         out_shape=jax.ShapeDtypeStruct((parts, rows, width), jnp.bfloat16),
         scratch_shapes=[pltpu.VMEM((parts, rows, width), jnp.float32)],
         cost_estimate=pl.CostEstimate(
-            flops=6 * groups * parts * rows * units * width,
+            flops=6 * parts * rows * units * width,
             bytes_accessed=2 * (2 * x.size + weights.size),
-            transcendentals=groups * rows * units,
+            transcendentals=rows * units,
         ),
         name="expert_mlp",
-    )(x, weights)
+    )(x, weights, weights, weights)
 
 
 fs = ("fh", "fl")
@@ -106,13 +112,12 @@
     got = lax.all_to_all(
         jnp.concatenate(pieces, axis=1), fs, split_axis=0, concat_axis=0, tiled=True
     )
-    units = places * own
-    got = got.reshape(places, 3, own, width).transpose(1, 0, 2, 3).reshape(3 * units, width)
-    whole = lax.all_gather(got, ("grp", "tp"), axis=0, tiled=False)
+    units = places * unit_rows
     served = lax.all_gather(got, "grp", axis=0, tiled=False)
-    served = served.reshape(groups, 3, places, own, width).transpose(1, 2, 0, 3, 4)
-    served = served.reshape(3, 1, groups * units, width)
-    gate_new, up_new, down_new = served[0], served[1], served[2]
+    served = served.reshape(groups, places, 3, own, width).transpose(2, 1, 0, 3, 4)
+    served = served.reshape(3 * units, width)
+    whole = lax.all_gather(served, "tp", axis=0, tiled=False)
+    gate_new, up_new, down_new = (served[None, i * units : (i + 1) * units] for i in range(3))
 
     block = jnp.concatenate(
         [
@@ -122,13 +127,9 @@
         ],
         axis=1,
     )
+    block, served = lax.optimization_barrier((block, served))
     block = lax.all_gather(block, "fh", axis=0, tiled=True)
     block = jnp.pad(block, ((0, 0), (0, width)))
-    block = lax.all_gather(block, "fl", axis=0, tiled=True)
-    block = block.reshape(lax.axis_size("fl"), lax.axis_size("fh"), unit_rows, 4 * width)
-    block = block.transpose(1, 0, 2, 3).reshape(places * unit_rows, 4 * width)
-    shared_g, shared_u, shared_d = (block[:, i * width : (i + 1) * width] for i in range(3))
-    units = places * unit_rows
 
     values = tokens.astype(jnp.float32)
     totals = lax.psum(jnp.sum(values * values, axis=1), "tp")
@@ -155,16 +156,22 @@
     outgoing = jnp.dot(placing, normed, preferred_element_type=jnp.float32)
     outgoing = outgoing.astype(jnp.bfloat16).reshape(experts, capacity, width)
     incoming = lax.all_to_all(outgoing, fs, split_axis=0, concat_axis=0, tiled=True)
+    incoming, block = lax.optimization_barrier((incoming, block))
+    block = lax.all_gather(block, "fl", axis=0, tiled=True)
     chunk = places * capacity // parts
     gathered = lax.all_to_all(
         incoming.reshape(parts, chunk, width), "tp", split_axis=0, concat_axis=0, tiled=True
     )
     produced = expert_mlp(gathered, whole)
     produced = lax.all_to_all(produced, "tp", split_axis=0, concat_axis=0, tiled=True)
+    produced, block = lax.optimization_barrier((produced, block))
     returned = lax.all_to_all(
         produced.reshape(places, capacity, width), fs, split_axis=0, concat_axis=0, tiled=True
     )
     returned = returned.reshape(experts * capacity, width)
+    block = block.reshape(lax.axis_size("fl"), lax.axis_size("fh"), unit_rows, 4 * width)
+    block = block.transpose(1, 0, 2, 3).reshape(units, 4 * width)
+    shared_g, shared_u, shared_d = (block[:, i * width : (i + 1) * width] for i in range(3))
 
     share_units = units // parts
     both = jnp.concatenate(

time: 529 us -> 429 us (0.81)
  the two profiles are of different devices: /device:TPU:33 before, /device:TPU:34 now
where the time goes in v4:
time: 429 us; the launch traced here: 428 us
  blocking collectives  256 us (60%)
  waiting for transfers between devices  109 us (25%)
  starting transfers between devices  28.4 us (7%)
  between operations  14.1 us (3%)
  Pallas kernels  8.01 us (2%)
  local copies, waits for them, and re-layouts  6.91 us (2%)
    all_gather x1, blocking collectives, layer(): block = lax.all_gather(block, 'fh', axis=0, tiled=True)  103 us
    all_to_all x1, blocking collectives, layer(): lax.all_to_all(jnp.concatenate(pieces, axis=1), fs, split_axis=0, concat_...  98.7 us
    reduce_scatter x1, waiting for transfers between devices, layer(): lax.psum_scatter(partial.reshape(tok_rows, parts, 2 * share_units).transp...  44.9 us
    all_gather x1, waiting for transfers between devices, layer(): block = lax.all_gather(block, 'fl', axis=0, tiled=True)  35.2 us
    all_to_all x1, waiting for transfers between devices, layer(): lax.all_to_all(produced.reshape(places, capacity, width), fs, split_axis=...  29 us
    all_to_all x1, blocking collectives, layer(): lax.all_to_all(incoming.reshape(parts, chunk, width), 'tp', split_axis=0,...  19.9 us
    all_to_all x1, starting transfers between devices, layer(): lax.all_to_all(produced.reshape(places, capacity, width), fs, split_axis=...  15.9 us
    all_gather x1, blocking collectives, layer(): shared_hidden = lax.all_gather(shared_hidden, 'tp', axis=1, tiled=True)  14 us
  transfers between devices with their start and end apart: 6, of which 3 were waited for; matrix products, arithmetic and copies ran while one was open for 2% of the time, Pallas kernels for 2%

profile of v4, /device:TPU:34, one launch (start us, length us, event | category | flops | bytes accessed | tf_op | source)
XLA Modules:
  0.0 427.9 jit_solution(4759073901047216415)
XLA Ops:
  7.2 0.0 copy-start
  7.2 0.1 all-gather.4.cloned.1.call-start
  7.3 1.0 copy-done
  8.2 1.1 multiply_convert_fusion.1
  9.4 98.7 %all_to_all.25 = bf16[32,24,256]{2,1,0:T(8,128)(2,1)S(1)} all-to-all(bf16[32,24,256]{2,1,0:T(8,128)(2,1)S(1)} %pad_maximum_fusion.1), channel_id=1, replica_groups=mesh['grp'=2,'fh'=4,'fl'=8,'tp'=8] {'fh','fl'}, dimensions={0} | all-to-all | bytes 786432 | tf_op jit(solution)/shard_map/all_to_all | solution.py:112
  108.1 0.0 copy-start.6
  108.1 0.0 copy-start.5
  108.1 10.0 %all-gather = bf16[64,24,256]{2,1,0:T(8,128)(2,1)S(1)} all-gather(bf16[32,24,256]{2,1,0:T(8,128)(2,1)S(1)} %all_to_all.25), channel_id=2, replica_groups=mesh['grp'=2,'fh'=4,'fl'=8,'tp'=8] {'grp'}, dimensions={0}, use_global_device_ids=true | all-gather | bytes 1179648 | tf_op jit(solution)/shard_map/all_gather | solution.py:116
  118.1 1.0 copy.33
  119.1 0.1 all-gather.4.cloned.1.call-update
  119.2 0.1 eq.45
  119.3 0.0 copy-done.6
  119.3 0.1 fusion.3
  119.5 0.0 copy-start.9
  119.5 0.3 bitcast_compare_fusion
  119.8 0.0 copy-done.5
  119.8 0.0 copy-start.7
  119.8 0.0 copy-start.8
  119.8 0.0 copy-start.11
  119.9 0.1 fusion.11
  120.0 10.1 %psum.7 = f32[192]{0:T(256)S(1)} all-reduce(f32[192]{0:T(256)S(1)} %fusion.11), channel_id=1, replica_groups=mesh['grp'=2,'fh'=4,'fl'=8,'tp'=8] {'tp'}, use_global_device_ids=true, to_apply=%region_3.4 | all-reduce | flops 192 | bytes 1536 | tf_op jit(solution)/shard_map/psum | solution.py:135
  130.1 1.4 convolution_convert_fusion
  131.5 6.8 %all-to-all-start = ((bf16[32,56,256]{2,1,0:T(8,128)(2,1)}), bf16[32,56,256]{2,1,0:T(8,128)(2,1)S(1)}, u32[]{:S(2)}, u32[]{:S(2)}) async-start(bf16[32,56,256]{2,1,0:T(8,128)(2,1)} %bitcast.3), calls=%async_computation | async-start | bytes 1835008 | tf_op jit(solution)/shard_map/all_to_all | solution.py:158
  138.3 0.1 all-gather.6.cloned.1.call-start
  138.4 0.0 copy-done.9
  138.4 0.0 copy-done.7
  138.4 0.0 copy-done.8
  138.4 0.0 copy-done.11
  138.4 102.9 %all_gather.18 = bf16[64,768]{1,0:T(8,128)(2,1)S(1)} all-gather(bf16[16,768]{1,0:T(8,128)(2,1)S(1)} %pad_maximum_fusion.2), channel_id=1, replica_groups=mesh['grp'=2,'fh'=4,'fl'=8,'tp'=8] {'fh'}, dimensions={0}, use_global_device_ids=true | all-gather | bytes 122880 | tf_op jit(solution)/shard_map/all_gather | solution.py:131
  241.4 0.7 pad.4
  242.0 0.0 all-to-all-done
  242.0 0.1 all-gather.6.cloned.1.call-update
  242.1 19.9 %all_to_all.26.x_ref = bf16[8,224,256]{2,1,0:T(8,128)(2,1)} all-to-all(bf16[8,224,256]{2,1,0:T(8,128)(2,1)S(1)} %bitcast.47), channel_id=1, replica_groups=mesh['grp'=2,'fh'=4,'fl'=8,'tp'=8] {'tp'}, dimensions={0} | all-to-all | bytes 1835008 | tf_op jit(solution)/shard_map/all_to_all | solution.py:162
  262.0 8.0 %expert_mlp.1 = bf16[8,224,256]{2,1,0:T(8,128)(2,1)} custom-call(bf16[8,224,256]{2,1,0:T(8,128)(2,1)} %all_to_all.26.x_ref, bf16[8,1536,256]{2,1,0:T(8,128)(2,1)} %all-gather.4.cloned.1.call-done.gate_ref.up_ref.down_ref, bf16[8,1536,256]{2,1,0:T(8,128)(2,1)} %all-gather.4.cloned.1.call-done.gate_ref.up_ref.down_ref, ...), custom_call_target="tpu_custom_call" | custom-call | flops 1409286144 | bytes 8126464 | tf_op jit(solution)/shard_map/expert_mlp/pallas_call | solution.py:57
  270.0 5.6 %all-to-all-start.3 = ((bf16[8,224,256]{2,1,0:T(8,128)(2,1)}), bf16[8,224,256]{2,1,0:T(8,128)(2,1)}, u32[]{:S(2)}, u32[]{:S(2)}) async-start(bf16[8,224,256]{2,1,0:T(8,128)(2,1)} %expert_mlp.1), calls=%async_computation.3 | async-start | bytes 1835008 | tf_op jit(solution)/shard_map/all_to_all | solution.py:166
  275.6 35.2 %all-gather.6.cloned.1.call-done = bf16[512,1024]{1,0:T(8,128)(2,1)} async-done(((bf16[64,1024]{1,0:T(8,128)(2,1)}), bf16[512,1024]{1,0:T(8,128)(2,1)}) %all-gather.6.cloned.1.call-update) | async-done | bytes 1048592 | tf_op jit(solution)/shard_map/all_gather | solution.py:160
  310.8 0.0 all-to-all-done.3
  310.8 15.9 %all-to-all-start.4 = ((bf16[32,56,256]{2,1,0:T(8,128)(2,1)}), bf16[32,56,256]{2,1,0:T(8,128)(2,1)S(1)}, u32[]{:S(2)}, u32[]{:S(2)}) async-start(bf16[32,56,256]{2,1,0:T(8,128)(2,1)} %bitcast.8), calls=%async_computation.4 | async-start | bytes 1835008 | tf_op jit(solution)/shard_map/all_to_all | solution.py:168
  326.7 0.1 reduce-scatter.2.cloned.1.call-start
  326.8 0.0 copy-done.1
  326.8 0.1 copy.34
  326.9 0.1 fusion.18
  326.9 0.0 copy-start.3
  326.9 0.0 copy-start.4
  327.0 0.0 copy-start.2
  327.0 0.0 copy-start.10
  327.0 0.3 fusion
  327.4 0.8 copy.42
  328.2 0.1 reduce-scatter.2.cloned.1.call-update
  328.3 0.0 copy-done.10
  328.3 0.1 fusion.19
  328.4 0.0 copy-done.3
  328.4 0.0 copy-done.4
  328.4 0.7 copy.37
  329.1 0.7 copy.38
  329.9 0.7 copy.39
  330.6 44.9 %reduce-scatter.2.cloned.1.call-done = bf16[1,192,128]{2,1,0:T(8,128)(2,1)} async-done(((bf16[8,192,128]{2,1,0:T(8,128)(2,1)}), bf16[1,192,128]{2,1,0:T(8,128)(2,1)}) %reduce-scatter.2.cloned.1.call-update) | async-done | bytes 49168 | tf_op jit(solution)/shard_map/reduce_scatter | solution.py:182
  375.5 0.9 copy.36
  376.4 14.0 %all_gather.23 = bf16[192,512]{0,1:T(8,128)(2,1)S(1)} all-gather(bf16[192,64]{0,1:T(8,128)(2,1)S(1)} %fusion.13), channel_id=1, replica_groups=mesh['grp'=2,'fh'=4,'fl'=8,'tp'=8] {'tp'}, dimensions={1}, use_global_device_ids=true | all-gather | bytes 221184 | tf_op jit(solution)/shard_map/all_gather | solution.py:191
  390.4 29.0 %all-to-all-done.4 = bf16[32,56,256]{2,1,0:T(8,128)(2,1)S(1)} async-done(((bf16[32,56,256]{2,1,0:T(8,128)(2,1)}), bf16[32,56,256]{2,1,0:T(8,128)(2,1)S(1)}, u32[]{:S(2)}, u32[]{:S(2)}) %all-to-all-start.4) | async-done | bytes 917536 | tf_op jit(solution)/shard_map/all_to_all | solution.py:168
  419.5 0.5 convolution_bitcast_fusion
  420.0 0.5 fusion.1
  420.5 0.0 copy-done.2
  420.5 0.9 fusion.2
  (15 shorter events, 0.2 us)
Async XLA Ops:
  7.2 1.0 copy-start
  7.2 254.8 %all-gather.4.cloned.1.call-start = ((), (), s32[]{:S(2)}) async-start(), calls=%async_computation.6 | async-start | bytes 7077888 | tf_op jit(solution)/shard_map/all_gather | solution.py:119
  108.1 11.2 %copy-start.6 = (s32[192,8]{0,1:T(8,128)S(1)}, s32[192,8]{0,1:T(8,128)}, u32[]{:S(2)}) copy-start(s32[192,8]{0,1:T(8,128)} %param.11) | copy-start | bytes 18436
  108.1 11.7 %copy-start.5 = (bf16[192,256]{1,0:T(8,128)(2,1)S(1)}, bf16[192,256]{1,0:T(8,128)(2,1)}, u32[]{:S(2)}) copy-start(bf16[192,256]{1,0:T(8,128)(2,1)} %param.10) | copy-start | bytes 294916
  119.5 18.9 %copy-start.9 = (f32[16,256]{1,0:T(8,128)S(1)}, f32[16,256]{1,0:T(8,128)}, u32[]{:S(2)}) copy-start(f32[16,256]{1,0:T(8,128)} %param.19) | copy-start | bytes 49156
  119.8 18.6 %copy-start.7 = (f32[16,256]{1,0:T(8,128)S(1)}, f32[16,256]{1,0:T(8,128)}, u32[]{:S(2)}) copy-start(f32[16,256]{1,0:T(8,128)} %param.17) | copy-start | bytes 49156
  119.8 18.6 %copy-start.8 = (f32[16,256]{1,0:T(8,128)S(1)}, f32[16,256]{1,0:T(8,128)}, u32[]{:S(2)}) copy-start(f32[16,256]{1,0:T(8,128)} %param.18) | copy-start | bytes 49156
  119.8 18.6 %copy-start.11 = (f32[256]{0:T(256)S(1)}, f32[256]{0:T(256)}, u32[]{:S(2)}) copy-start(f32[256]{0:T(256)} %param.13) | copy-start | bytes 3076
  131.5 110.5 %all-to-all-start = ((bf16[32,56,256]{2,1,0:T(8,128)(2,1)}), bf16[32,56,256]{2,1,0:T(8,128)(2,1)S(1)}, u32[]{:S(2)}, u32[]{:S(2)}) async-start(bf16[32,56,256]{2,1,0:T(8,128)(2,1)} %bitcast.3), calls=%async_computation | async-start | bytes 1835008 | tf_op jit(solution)/shard_map/all_to_all | solution.py:158
  138.3 172.5 %all-gather.6.cloned.1.call-start = ((), (), s32[]{:S(2)}) async-start(), calls=%async_computation.7 | async-start | bytes 1179648 | tf_op jit(solution)/shard_map/all_gather | solution.py:160
  270.0 40.8 %all-to-all-start.3 = ((bf16[8,224,256]{2,1,0:T(8,128)(2,1)}), bf16[8,224,256]{2,1,0:T(8,128)(2,1)}, u32[]{:S(2)}, u32[]{:S(2)}) async-start(bf16[8,224,256]{2,1,0:T(8,128)(2,1)} %expert_mlp.1), calls=%async_computation.3 | async-start | bytes 1835008 | tf_op jit(solution)/shard_map/all_to_all | solution.py:166
  310.8 16.0 %copy-start.1 = (bf16[512,1024]{1,0:T(8,128)(2,1)S(1)}, bf16[512,1024]{1,0:T(8,128)(2,1)}, u32[]{:S(2)}) copy-start(bf16[512,1024]{1,0:T(8,128)(2,1)} %all-gather.6.cloned.1.call-done) | copy-start | bytes 3145732
  310.8 108.7 %all-to-all-start.4 = ((bf16[32,56,256]{2,1,0:T(8,128)(2,1)}), bf16[32,56,256]{2,1,0:T(8,128)(2,1)S(1)}, u32[]{:S(2)}, u32[]{:S(2)}) async-start(bf16[32,56,256]{2,1,0:T(8,128)(2,1)} %bitcast.8), calls=%async_computation.4 | async-start | bytes 1835008 | tf_op jit(solution)/shard_map/all_to_all | solution.py:168
  326.7 48.8 %reduce-scatter.2.cloned.1.call-start = ((), (), s32[]{:S(2)}) async-start(), calls=%async_computation.8 | async-start | bytes 442368 | tf_op jit(solution)/shard_map/reduce_scatter | solution.py:182
  326.9 1.5 copy-start.3
  326.9 1.5 copy-start.4
  327.0 93.5 %copy-start.2 = (bf16[512,256]{1,0:T(8,128)(2,1)}, bf16[512,256]{1,0:T(8,128)(2,1)S(1)}, u32[]{:S(2)}) copy-start(bf16[512,256]{1,0:T(8,128)(2,1)S(1)} %get-tuple-element.15) | copy-start | bytes 786436
  327.0 1.3 copy-start.10
Sparse Core Ops, SparseCore 0:
  119.3 39.8 all-gather.3
  242.2 68.5 all-gather.5
  330.3 45.0 reduce-scatter.1

commit v5 on v4

--- a/solution.py
+++ b/solution.py
@@ -75,7 +75,7 @@
     )(x, weights, weights, weights)
 
 
-fs = ("fh", "fl")
+fs = ("fh", "fm", "fl")
 
 
 def layer(
@@ -127,6 +127,7 @@
         ],
         axis=1,
     )
+    block = lax.all_gather(block, "fm", axis=0, tiled=True)
     block, served = lax.optimization_barrier((block, served))
     block = lax.all_gather(block, "fh", axis=0, tiled=True)
     block = jnp.pad(block, ((0, 0), (0, width)))
@@ -169,8 +170,9 @@
         produced.reshape(places, capacity, width), fs, split_axis=0, concat_axis=0, tiled=True
     )
     returned = returned.reshape(experts * capacity, width)
-    block = block.reshape(lax.axis_size("fl"), lax.axis_size("fh"), unit_rows, 4 * width)
-    block = block.transpose(1, 0, 2, 3).reshape(units, 4 * width)
+    sizes = [lax.axis_size(a) for a in ("fl", "fh", "fm")]
+    block = block.reshape(*sizes, unit_rows, 4 * width)
+    block = block.transpose(1, 2, 0, 3, 4).reshape(units, 4 * width)
     shared_g, shared_u, shared_d = (block[:, i * width : (i + 1) * width] for i in range(3))
 
     share_units = units // parts
@@ -210,9 +212,10 @@
 
 def solution(mesh):
     count = mesh.shape["fs"]
-    low = 8 if count % 8 == 0 else 1
+    low = 4 if count % 8 == 0 else 1
+    mid = 2 if count % 8 == 0 else 1
     cut = Mesh(
-        mesh.devices.reshape(mesh.shape["grp"], count // low, low, mesh.shape["tp"]),
+        mesh.devices.reshape(mesh.shape["grp"], -1, mid, low, mesh.shape["tp"]),
         ("grp",) + fs + ("tp",),
     )
     line = ("grp",) + fs

time: 429 us -> 435 us (1.014)
  the two profiles are of different devices: /device:TPU:34 before, /device:TPU:33 now
where the time goes in v5:
time: 435 us
  blocking collectives  251 us (58%)
  waiting for transfers between devices  104 us (24%)
  starting transfers between devices  44.5 us (10%)
  between operations  14.1 us (3%)
  Pallas kernels  8.02 us (2%)
  local copies, waits for them, and re-layouts  7.95 us (2%)
    all_to_all x1, blocking collectives, layer(): lax.all_to_all(jnp.concatenate(pieces, axis=1), fs, split_axis=0, concat_...  97.4 us
    all_gather x1, blocking collectives, layer(): block = lax.all_gather(block, 'fm', axis=0, tiled=True)  72.3 us
    reduce_scatter x1, waiting for transfers between devices, layer(): lax.psum_scatter(partial.reshape(tok_rows, parts, 2 * share_units).transp...  47.6 us
    all_gather x1, blocking collectives, layer(): block = lax.all_gather(block, 'fh', axis=0, tiled=True)  42.1 us
    all_to_all x1, waiting for transfers between devices, layer(): lax.all_to_all(produced.reshape(places, capacity, width), fs, split_axis=...  28.9 us
    all_to_all x1, starting transfers between devices, layer(): lax.all_to_all(produced.reshape(places, capacity, width), fs, split_axis=...  21.2 us
    psum x1, blocking collectives, layer(): totals = lax.psum(jnp.sum(values * values, axis=1), 'tp')  15.5 us
    all_gather x1, blocking collectives, layer(): shared_hidden = lax.all_gather(shared_hidden, 'tp', axis=1, tiled=True)  13.9 us
  transfers between devices with their start and end apart: 7, of which 5 were waited for; matrix products, arithmetic and copies ran while one was open for 2% of the time, Pallas kernels for 2%

profile of v5, /device:TPU:33, one launch (start us, length us, event | category | flops | bytes accessed | tf_op | source)
XLA Modules:
  0.0 434.6 jit_solution(13927547518897760414)
XLA Ops:
  7.2 0.0 copy-start
  7.2 0.1 all-gather.4.cloned.1.call-start
  7.3 1.0 copy-done
  8.2 1.1 multiply_convert_fusion.1
  9.4 97.4 %all_to_all.25 = bf16[32,24,256]{2,1,0:T(8,128)(2,1)S(1)} all-to-all(bf16[32,24,256]{2,1,0:T(8,128)(2,1)S(1)} %pad_maximum_fusion.1), channel_id=1, replica_groups=mesh['grp'=2,'fh'=4,'fm'=2,'fl'=4,'tp'=8] {'fh','fm','fl'}, dimensions={0} | all-to-all | bytes 786432 | tf_op jit(solution)/shard_map/all_to_all | solution.py:112
  106.8 9.4 %all-gather = bf16[64,24,256]{2,1,0:T(8,128)(2,1)S(1)} all-gather(bf16[32,24,256]{2,1,0:T(8,128)(2,1)S(1)} %all_to_all.25), channel_id=2, replica_groups=mesh['grp'=2,'fh'=4,'fm'=2,'fl'=4,'tp'=8] {'grp'}, dimensions={0}, use_global_device_ids=true | all-gather | bytes 1179648 | tf_op jit(solution)/shard_map/all_gather | solution.py:116
  116.2 1.0 copy.33
  117.2 0.1 all-gather.4.cloned.1.call-update
  117.3 0.1 eq.45
  117.4 0.0 copy-done.7
  117.4 0.1 fusion.3
  117.6 0.3 bitcast_compare_fusion
  117.9 0.0 copy-done.6
  117.9 0.0 copy-start.8
  117.9 0.0 copy-start.9
  117.9 0.0 copy-start.12
  118.0 0.1 fusion.11
  118.1 15.5 %psum.7 = f32[192]{0:T(256)S(1)} all-reduce(f32[192]{0:T(256)S(1)} %fusion.11), channel_id=1, replica_groups=mesh['grp'=2,'fh'=4,'fm'=2,'fl'=4,'tp'=8] {'tp'}, use_global_device_ids=true, to_apply=%region_3.4 | all-reduce | flops 192 | bytes 1536 | tf_op jit(solution)/shard_map/psum | solution.py:136
  133.6 1.4 convolution_convert_fusion
  135.0 5.5 %all-to-all-start = ((bf16[32,56,256]{2,1,0:T(8,128)(2,1)}), bf16[32,56,256]{2,1,0:T(8,128)(2,1)}, u32[]{:S(2)}, u32[]{:S(2)}) async-start(bf16[32,56,256]{2,1,0:T(8,128)(2,1)} %bitcast.3), calls=%async_computation | async-start | bytes 1835008 | tf_op jit(solution)/shard_map/all_to_all | solution.py:159
  140.5 0.0 copy-done.10
  140.5 0.0 copy-done.8
  140.5 0.0 copy-done.9
  140.5 0.0 copy-done.12
  140.5 72.3 %all_gather.21 = bf16[32,768]{1,0:T(8,128)(2,1)S(1)} all-gather(bf16[16,768]{1,0:T(8,128)(2,1)S(1)} %pad_maximum_fusion.2), channel_id=1, replica_groups=mesh['grp'=2,'fh'=4,'fm'=2,'fl'=4,'tp'=8] {'fm'}, dimensions={0}, use_global_device_ids=true | all-gather | bytes 73728 | tf_op jit(solution)/shard_map/all_gather | solution.py:130
  212.8 42.1 %all_gather.22 = bf16[128,768]{1,0:T(8,128)(2,1)S(1)} all-gather(bf16[32,768]{1,0:T(8,128)(2,1)S(1)} %all_gather.21), channel_id=1, replica_groups=mesh['grp'=2,'fh'=4,'fm'=2,'fl'=4,'tp'=8] {'fh'}, dimensions={0}, use_global_device_ids=true | all-gather | bytes 245760 | tf_op jit(solution)/shard_map/all_gather | solution.py:132
  254.9 0.7 pad.4
  255.6 0.0 all-to-all-done
  255.6 12.7 %all-to-all-start.1 = ((bf16[8,224,256]{2,1,0:T(8,128)(2,1)}), bf16[8,224,256]{2,1,0:T(8,128)(2,1)S(1)}, u32[]{:S(2)}, u32[]{:S(2)}) async-start(bf16[8,224,256]{2,1,0:T(8,128)(2,1)} %bitcast.4), calls=%async_computation.1 | async-start | bytes 1835008 | tf_op jit(solution)/shard_map/all_to_all | solution.py:163
  268.3 0.0 all-gather.6.cloned.1.call-start
  268.3 0.8 all-gather.6.cloned.1.call-update
  269.1 12.9 %all-to-all-done.1.x_ref = bf16[8,224,256]{2,1,0:T(8,128)(2,1)S(1)} async-done(((bf16[8,224,256]{2,1,0:T(8,128)(2,1)}), bf16[8,224,256]{2,1,0:T(8,128)(2,1)S(1)}, u32[]{:S(2)}, u32[]{:S(2)}) %all-to-all-start.1) | async-done | bytes 917536 | tf_op jit(solution)/shard_map/all_to_all | solution.py:163
  282.0 1.0 copy-done.1
  282.9 8.0 %expert_mlp.1 = bf16[8,224,256]{2,1,0:T(8,128)(2,1)} custom-call(bf16[8,224,256]{2,1,0:T(8,128)(2,1)} %copy-done.1, bf16[8,1536,256]{2,1,0:T(8,128)(2,1)} %all-gather.4.cloned.1.call-done.gate_ref.up_ref.down_ref, bf16[8,1536,256]{2,1,0:T(8,128)(2,1)} %all-gather.4.cloned.1.call-done.gate_ref.up_ref.down_ref, ...), custom_call_target="tpu_custom_call" | custom-call | flops 1409286144 | bytes 8126464 | tf_op jit(solution)/shard_map/expert_mlp/pallas_call | solution.py:57
  290.9 5.1 %all-to-all-start.3 = ((bf16[8,224,256]{2,1,0:T(8,128)(2,1)}), bf16[8,224,256]{2,1,0:T(8,128)(2,1)}, u32[]{:S(2)}, u32[]{:S(2)}) async-start(bf16[8,224,256]{2,1,0:T(8,128)(2,1)} %expert_mlp.1), calls=%async_computation.3 | async-start | bytes 1835008 | tf_op jit(solution)/shard_map/all_to_all | solution.py:167
  296.0 13.3 %all-gather.6.cloned.1.call-done = bf16[512,1024]{1,0:T(8,128)(2,1)} async-done(((bf16[128,1024]{1,0:T(8,128)(2,1)}), bf16[512,1024]{1,0:T(8,128)(2,1)}) %all-gather.6.cloned.1.call-update) | async-done | bytes 1048592 | tf_op jit(solution)/shard_map/all_gather | solution.py:161
  309.4 0.4 all-to-all-done.3
  309.8 21.2 %all-to-all-start.4 = ((bf16[32,56,256]{2,1,0:T(8,128)(2,1)}), bf16[32,56,256]{2,1,0:T(8,128)(2,1)S(1)}, u32[]{:S(2)}, u32[]{:S(2)}) async-start(bf16[32,56,256]{2,1,0:T(8,128)(2,1)} %bitcast.8), calls=%async_computation.4 | async-start | bytes 1835008 | tf_op jit(solution)/shard_map/all_to_all | solution.py:169
  331.0 0.1 reduce-scatter.2.cloned.1.call-start
  331.0 0.0 copy-done.2
  331.0 0.1 copy.34
  331.1 0.1 fusion.18
  331.2 0.0 copy-start.4
  331.2 0.0 copy-start.5
  331.2 0.0 copy-start.3
  331.2 0.0 copy-start.11
  331.3 0.3 fusion
  331.6 0.8 copy.42
  332.5 0.1 reduce-scatter.2.cloned.1.call-update
  332.5 0.0 copy-done.11
  332.6 0.1 fusion.19
  332.7 0.0 copy-done.4
  332.7 0.0 copy-done.5
  332.7 0.7 copy.37
  333.4 0.7 copy.38
  334.1 0.7 copy.39
  334.9 47.6 %reduce-scatter.2.cloned.1.call-done = bf16[1,192,128]{2,1,0:T(8,128)(2,1)} async-done(((bf16[8,192,128]{2,1,0:T(8,128)(2,1)}), bf16[1,192,128]{2,1,0:T(8,128)(2,1)}) %reduce-scatter.2.cloned.1.call-update) | async-done | bytes 49168 | tf_op jit(solution)/shard_map/reduce_scatter | solution.py:184
  382.5 0.9 copy.36
  383.4 13.9 %all_gather.27 = bf16[192,512]{0,1:T(8,128)(2,1)S(1)} all-gather(bf16[192,64]{0,1:T(8,128)(2,1)S(1)} %fusion.13), channel_id=1, replica_groups=mesh['grp'=2,'fh'=4,'fm'=2,'fl'=4,'tp'=8] {'tp'}, dimensions={1}, use_global_device_ids=true | all-gather | bytes 221184 | tf_op jit(solution)/shard_map/all_gather | solution.py:193
  397.3 28.9 %all-to-all-done.4 = bf16[32,56,256]{2,1,0:T(8,128)(2,1)S(1)} async-done(((bf16[32,56,256]{2,1,0:T(8,128)(2,1)}), bf16[32,56,256]{2,1,0:T(8,128)(2,1)S(1)}, u32[]{:S(2)}, u32[]{:S(2)}) %all-to-all-start.4) | async-done | bytes 917536 | tf_op jit(solution)/shard_map/all_to_all | solution.py:169
  426.2 0.5 convolution_bitcast_fusion
  426.7 0.5 fusion.1
  427.2 0.0 copy-done.3
  427.2 0.9 fusion.2
  (19 shorter events, 0.2 us)
Async XLA Ops:
  7.2 1.0 copy-start
  7.2 274.8 %all-gather.4.cloned.1.call-start = ((), (), s32[]{:S(2)}) async-start(), calls=%async_computation.6 | async-start | bytes 7077888 | tf_op jit(solution)/shard_map/all_gather | solution.py:119
  106.8 10.6 %copy-start.7 = (s32[192,8]{0,1:T(8,128)S(1)}, s32[192,8]{0,1:T(8,128)}, u32[]{:S(2)}) copy-start(s32[192,8]{0,1:T(8,128)} %param.11) | copy-start | bytes 18436
  106.8 11.1 %copy-start.6 = (bf16[192,256]{1,0:T(8,128)(2,1)S(1)}, bf16[192,256]{1,0:T(8,128)(2,1)}, u32[]{:S(2)}) copy-start(bf16[192,256]{1,0:T(8,128)(2,1)} %param.10) | copy-start | bytes 294916
  117.6 22.9 %copy-start.10 = (f32[16,256]{1,0:T(8,128)S(1)}, f32[16,256]{1,0:T(8,128)}, u32[]{:S(2)}) copy-start(f32[16,256]{1,0:T(8,128)} %param.19) | copy-start | bytes 49156
  117.9 22.6 %copy-start.8 = (f32[16,256]{1,0:T(8,128)S(1)}, f32[16,256]{1,0:T(8,128)}, u32[]{:S(2)}) copy-start(f32[16,256]{1,0:T(8,128)} %param.17) | copy-start | bytes 49156
  117.9 22.6 %copy-start.9 = (f32[16,256]{1,0:T(8,128)S(1)}, f32[16,256]{1,0:T(8,128)}, u32[]{:S(2)}) copy-start(f32[16,256]{1,0:T(8,128)} %param.18) | copy-start | bytes 49156
  117.9 22.6 %copy-start.12 = (f32[256]{0:T(256)S(1)}, f32[256]{0:T(256)}, u32[]{:S(2)}) copy-start(f32[256]{0:T(256)} %param.13) | copy-start | bytes 3076
  135.0 120.6 %all-to-all-start = ((bf16[32,56,256]{2,1,0:T(8,128)(2,1)}), bf16[32,56,256]{2,1,0:T(8,128)(2,1)}, u32[]{:S(2)}, u32[]{:S(2)}) async-start(bf16[32,56,256]{2,1,0:T(8,128)(2,1)} %bitcast.3), calls=%async_computation | async-start | bytes 1835008 | tf_op jit(solution)/shard_map/all_to_all | solution.py:159
  255.6 26.3 %all-to-all-start.1 = ((bf16[8,224,256]{2,1,0:T(8,128)(2,1)}), bf16[8,224,256]{2,1,0:T(8,128)(2,1)S(1)}, u32[]{:S(2)}, u32[]{:S(2)}) async-start(bf16[8,224,256]{2,1,0:T(8,128)(2,1)} %bitcast.4), calls=%async_computation.1 | async-start | bytes 1835008 | tf_op jit(solution)/shard_map/all_to_all | solution.py:163
  268.3 41.1 %all-gather.6.cloned.1.call-start = ((), (), s32[]{:S(2)}) async-start(), calls=%async_computation.7 | async-start | bytes 1310720 | tf_op jit(solution)/shard_map/all_gather | solution.py:161
  281.9 1.0 copy-start.1
  290.9 18.8 %all-to-all-start.3 = ((bf16[8,224,256]{2,1,0:T(8,128)(2,1)}), bf16[8,224,256]{2,1,0:T(8,128)(2,1)}, u32[]{:S(2)}, u32[]{:S(2)}) async-start(bf16[8,224,256]{2,1,0:T(8,128)(2,1)} %expert_mlp.1), calls=%async_computation.3 | async-start | bytes 1835008 | tf_op jit(solution)/shard_map/all_to_all | solution.py:167
  309.4 21.7 %copy-start.2 = (bf16[512,1024]{1,0:T(8,128)(2,1)S(1)}, bf16[512,1024]{1,0:T(8,128)(2,1)}, u32[]{:S(2)}) copy-start(bf16[512,1024]{1,0:T(8,128)(2,1)} %all-gather.6.cloned.1.call-done) | copy-start | bytes 3145732
  309.8 116.4 %all-to-all-start.4 = ((bf16[32,56,256]{2,1,0:T(8,128)(2,1)}), bf16[32,56,256]{2,1,0:T(8,128)(2,1)S(1)}, u32[]{:S(2)}, u32[]{:S(2)}) async-start(bf16[32,56,256]{2,1,0:T(8,128)(2,1)} %bitcast.8), calls=%async_computation.4 | async-start | bytes 1835008 | tf_op jit(solution)/shard_map/all_to_all | solution.py:169
  331.0 51.5 %reduce-scatter.2.cloned.1.call-start = ((), (), s32[]{:S(2)}) async-start(), calls=%async_computation.8 | async-start | bytes 442368 | tf_op jit(solution)/shard_map/reduce_scatter | solution.py:184
  331.2 1.5 copy-start.4
  331.2 1.5 copy-start.5
  331.2 96.0 %copy-start.3 = (bf16[512,256]{1,0:T(8,128)(2,1)}, bf16[512,256]{1,0:T(8,128)(2,1)S(1)}, u32[]{:S(2)}) copy-start(bf16[512,256]{1,0:T(8,128)(2,1)S(1)} %get-tuple-element.15) | copy-start | bytes 786436
  331.2 1.3 copy-start.11
Sparse Core Ops, SparseCore 0:
  117.4 44.0 all-gather.3
  271.8 37.5 all-gather.5
  334.6 47.8 reduce-scatter.1

commit v6 on v4

--- a/solution.py
+++ b/solution.py
@@ -75,7 +75,7 @@
     )(x, weights, weights, weights)
 
 
-fs = ("fh", "fl")
+fs = ("fa", "fb", "fc", "fl")
 
 
 def layer(
@@ -127,8 +127,10 @@
         ],
         axis=1,
     )
+    block = lax.all_gather(block, "fa", axis=0, tiled=True)
     block, served = lax.optimization_barrier((block, served))
-    block = lax.all_gather(block, "fh", axis=0, tiled=True)
+    block = lax.all_gather(block, "fb", axis=0, tiled=True)
+    block = lax.all_gather(block, "fc", axis=0, tiled=True)
     block = jnp.pad(block, ((0, 0), (0, width)))
 
     values = tokens.astype(jnp.float32)
@@ -164,13 +166,13 @@
     )
     produced = expert_mlp(gathered, whole)
     produced = lax.all_to_all(produced, "tp", split_axis=0, concat_axis=0, tiled=True)
-    produced, block = lax.optimization_barrier((produced, block))
     returned = lax.all_to_all(
         produced.reshape(places, capacity, width), fs, split_axis=0, concat_axis=0, tiled=True
     )
     returned = returned.reshape(experts * capacity, width)
-    block = block.reshape(lax.axis_size("fl"), lax.axis_size("fh"), unit_rows, 4 * width)
-    block = block.transpose(1, 0, 2, 3).reshape(units, 4 * width)
+    sizes = [lax.axis_size(a) for a in fs[::-1]]
+    block = block.reshape(*sizes, unit_rows, 4 * width)
+    block = block.transpose(3, 2, 1, 0, 4, 5).reshape(units, 4 * width)
     shared_g, shared_u, shared_d = (block[:, i * width : (i + 1) * width] for i in range(3))
 
     share_units = units // parts
@@ -209,10 +211,9 @@
 
 
 def solution(mesh):
-    count = mesh.shape["fs"]
-    low = 8 if count % 8 == 0 else 1
+    pair = 2 if mesh.shape["fs"] % 8 == 0 else 1
     cut = Mesh(
-        mesh.devices.reshape(mesh.shape["grp"], count // low, low, mesh.shape["tp"]),
+        mesh.devices.reshape(mesh.shape["grp"], pair, pair, pair, -1, mesh.shape["tp"]),
         ("grp",) + fs + ("tp",),
     )
     line = ("grp",) + fs

time: 429 us -> 487 us (1.14)
  the two profiles are of different devices: /device:TPU:34 before, /device:TPU:33 now
where the time goes in v6:
time: 487 us; the launch traced here: 486 us
  blocking collectives  296 us (61%)
  waiting for transfers between devices  139 us (29%)
  between operations  15.9 us (3%)
  starting transfers between devices  14.3 us (3%)
  local copies, waits for them, and re-layouts  8.09 us (2%)
  Pallas kernels  7.95 us (2%)
    all_to_all x1, blocking collectives, layer(): lax.all_to_all(jnp.concatenate(pieces, axis=1), fs, split_axis=0, concat_...  97.4 us
    all_gather x1, blocking collectives, layer(): block = lax.all_gather(block, 'fa', axis=0, tiled=True)  96.5 us
    all_gather x1, waiting for transfers between devices, layer(): block = lax.all_gather(block, 'fl', axis=0, tiled=True)  96.5 us
    reduce_scatter x1, waiting for transfers between devices, layer(): lax.psum_scatter(partial.reshape(tok_rows, parts, 2 * share_units).transp...  41.5 us
    all_to_all x1, blocking collectives, layer(): lax.all_to_all(incoming.reshape(parts, chunk, width), 'tp', split_axis=0,...  19.3 us
    all_to_all x1, blocking collectives, layer(): lax.all_to_all(produced, 'tp', split_axis=0, concat_axis=0, tiled=True)  18.9 us
    psum x1, blocking collectives, layer(): totals = lax.psum(jnp.sum(values * values, axis=1), 'tp')  15.5 us
    all_gather x1, blocking collectives, layer(): block = lax.all_gather(block, 'fb', axis=0, tiled=True)  14.8 us
  transfers between devices with their start and end apart: 5, of which 2 were waited for; matrix products, arithmetic and copies ran while one was open for 2% of the time, Pallas kernels for 0%

profile of v6, /device:TPU:33, one launch (start us, length us, event | category | flops | bytes accessed | tf_op | source)
XLA Modules:
  0.0 486.5 jit_solution(9834209564790900915)
XLA Ops:
  8.0 0.0 copy-start
  8.1 0.1 all-gather.4.cloned.1.call-start
  8.1 1.0 copy-done
  9.1 1.1 multiply_convert_fusion.1
  10.2 97.4 %all_to_all.25 = bf16[32,24,256]{2,1,0:T(8,128)(2,1)S(1)} all-to-all(bf16[32,24,256]{2,1,0:T(8,128)(2,1)S(1)} %pad_maximum_fusion.1), channel_id=1, replica_groups=mesh['grp'=2,'fa'=2,'fb'=2,'fc'=2,'fl'=4,'tp'=8] {'fa','fb','fc','fl'}, dimensions={0} | all-to-all | bytes 786432 | tf_op jit(solution)/shard_map/all_to_all | solution.py:112
  107.6 0.0 copy-start.5
  107.6 0.0 copy-start.4
  107.6 9.4 %all-gather = bf16[64,24,256]{2,1,0:T(8,128)(2,1)S(1)} all-gather(bf16[32,24,256]{2,1,0:T(8,128)(2,1)S(1)} %all_to_all.25), channel_id=2, replica_groups=mesh['grp'=2,'fa'=2,'fb'=2,'fc'=2,'fl'=4,'tp'=8] {'grp'}, dimensions={0}, use_global_device_ids=true | all-gather | bytes 1179648 | tf_op jit(solution)/shard_map/all_gather | solution.py:116
  117.1 1.0 copy.33
  118.0 0.1 all-gather.4.cloned.1.call-update
  118.1 0.1 eq.45
  118.2 0.0 copy-done.5
  118.2 0.1 fusion.3
  118.4 0.0 copy-start.8
  118.4 0.3 bitcast_compare_fusion
  118.7 0.0 copy-done.4
  118.7 0.0 copy-start.6
  118.7 0.0 copy-start.7
  118.7 0.0 copy-start.10
  118.7 0.1 fusion.11
  118.9 15.5 %psum.7 = f32[192]{0:T(256)S(1)} all-reduce(f32[192]{0:T(256)S(1)} %fusion.11), channel_id=1, replica_groups=mesh['grp'=2,'fa'=2,'fb'=2,'fc'=2,'fl'=4,'tp'=8] {'tp'}, use_global_device_ids=true, to_apply=%region_3.4 | all-reduce | flops 192 | bytes 1536 | tf_op jit(solution)/shard_map/psum | solution.py:137
  134.3 1.4 convolution_convert_fusion
  135.8 5.1 %all-to-all-start = ((bf16[32,56,256]{2,1,0:T(8,128)(2,1)}), bf16[32,56,256]{2,1,0:T(8,128)(2,1)S(1)}, u32[]{:S(2)}, u32[]{:S(2)}) async-start(bf16[32,56,256]{2,1,0:T(8,128)(2,1)} %bitcast.3), calls=%async_computation | async-start | bytes 1835008 | tf_op jit(solution)/shard_map/all_to_all | solution.py:160
  140.9 0.0 copy-done.8
  140.9 0.0 copy-done.6
  140.9 0.0 copy-done.7
  140.9 0.0 copy-done.10
  141.0 96.5 %all_gather.24 = bf16[32,768]{1,0:T(8,128)(2,1)S(1)} all-gather(bf16[16,768]{1,0:T(8,128)(2,1)S(1)} %pad_maximum_fusion.2), channel_id=1, replica_groups=mesh['grp'=2,'fa'=2,'fb'=2,'fc'=2,'fl'=4,'tp'=8] {'fa'}, dimensions={0}, use_global_device_ids=true | all-gather | bytes 73728 | tf_op jit(solution)/shard_map/all_gather | solution.py:130
  237.5 14.8 %all_gather.25 = bf16[64,768]{1,0:T(8,128)(2,1)S(1)} all-gather(bf16[32,768]{1,0:T(8,128)(2,1)S(1)} %all_gather.24), channel_id=1, replica_groups=mesh['grp'=2,'fa'=2,'fb'=2,'fc'=2,'fl'=4,'tp'=8] {'fb'}, dimensions={0}, use_global_device_ids=true | all-gather | bytes 147456 | tf_op jit(solution)/shard_map/all_gather | solution.py:132
  252.4 10.4 %all_gather.26 = bf16[128,768]{1,0:T(8,128)(2,1)S(1)} all-gather(bf16[64,768]{1,0:T(8,128)(2,1)S(1)} %all_gather.25), channel_id=1, replica_groups=mesh['grp'=2,'fa'=2,'fb'=2,'fc'=2,'fl'=4,'tp'=8] {'fc'}, dimensions={0}, use_global_device_ids=true | all-gather | bytes 294912 | tf_op jit(solution)/shard_map/all_gather | solution.py:133
  262.7 0.7 pad.4
  263.5 0.0 all-to-all-done
  263.5 19.3 %all_to_all.26.x_ref = bf16[8,224,256]{2,1,0:T(8,128)(2,1)} all-to-all(bf16[8,224,256]{2,1,0:T(8,128)(2,1)S(1)} %bitcast.47), channel_id=1, replica_groups=mesh['grp'=2,'fa'=2,'fb'=2,'fc'=2,'fl'=4,'tp'=8] {'tp'}, dimensions={0} | all-to-all | bytes 1835008 | tf_op jit(solution)/shard_map/all_to_all | solution.py:164
  282.8 7.9 %expert_mlp.1 = bf16[8,224,256]{2,1,0:T(8,128)(2,1)} custom-call(bf16[8,224,256]{2,1,0:T(8,128)(2,1)} %all_to_all.26.x_ref, bf16[8,1536,256]{2,1,0:T(8,128)(2,1)} %all-gather.4.cloned.1.call-done.gate_ref.up_ref.down_ref, bf16[8,1536,256]{2,1,0:T(8,128)(2,1)} %all-gather.4.cloned.1.call-done.gate_ref.up_ref.down_ref, ...), custom_call_target="tpu_custom_call" | custom-call | flops 1409286144 | bytes 8126464 | tf_op jit(solution)/shard_map/expert_mlp/pallas_call | solution.py:57
  290.8 18.9 %all_to_all.27 = bf16[8,224,256]{2,1,0:T(8,128)(2,1)} all-to-all(bf16[8,224,256]{2,1,0:T(8,128)(2,1)} %expert_mlp.1), channel_id=1, replica_groups=mesh['grp'=2,'fa'=2,'fb'=2,'fc'=2,'fl'=4,'tp'=8] {'tp'}, dimensions={0} | all-to-all | bytes 1835008 | tf_op jit(solution)/shard_map/all_to_all | solution.py:168
  309.6 9.0 %all-to-all-start.4 = ((bf16[32,56,256]{2,1,0:T(8,128)(2,1)}), bf16[32,56,256]{2,1,0:T(8,128)(2,1)S(1)}, u32[]{:S(2)}, u32[]{:S(2)}) async-start(bf16[32,56,256]{2,1,0:T(8,128)(2,1)} %bitcast.8), calls=%async_computation.4 | async-start | bytes 1835008 | tf_op jit(solution)/shard_map/all_to_all | solution.py:169
  318.6 0.1 all-gather.6.cloned.1.call-start
  318.7 0.6 all-gather.6.cloned.1.call-update
  319.2 0.1 reduce-scatter.2.cloned.1.call-start
  319.3 96.5 %all-gather.6.cloned.1.call-done = bf16[512,1024]{1,0:T(8,128)(2,1)} async-done(((bf16[128,1024]{1,0:T(8,128)(2,1)}), bf16[512,1024]{1,0:T(8,128)(2,1)}) %all-gather.6.cloned.1.call-update) | async-done | bytes 1048592 | tf_op jit(solution)/shard_map/all_gather | solution.py:162
  415.8 1.3 copy.34
  417.1 0.1 fusion.18
  417.2 0.0 copy-start.2
  417.2 0.0 copy-start.3
  417.2 0.0 copy-start.1
  417.2 0.0 copy-start.9
  417.3 0.3 fusion
  417.6 0.8 copy.42
  418.4 0.1 reduce-scatter.2.cloned.1.call-update
  418.5 0.0 copy-done.9
  418.6 0.1 fusion.19
  418.6 0.0 copy-done.2
  418.6 0.0 copy-done.3
  418.7 0.7 copy.37
  419.4 0.7 copy.38
  420.1 0.7 copy.39
  420.8 41.5 %reduce-scatter.2.cloned.1.call-done = bf16[1,192,128]{2,1,0:T(8,128)(2,1)} async-done(((bf16[8,192,128]{2,1,0:T(8,128)(2,1)}), bf16[1,192,128]{2,1,0:T(8,128)(2,1)}) %reduce-scatter.2.cloned.1.call-update) | async-done | bytes 49168 | tf_op jit(solution)/shard_map/reduce_scatter | solution.py:184
  462.3 0.9 copy.36
  463.3 13.8 %all_gather.31 = bf16[192,512]{0,1:T(8,128)(2,1)S(1)} all-gather(bf16[192,64]{0,1:T(8,128)(2,1)S(1)} %fusion.13), channel_id=1, replica_groups=mesh['grp'=2,'fa'=2,'fb'=2,'fc'=2,'fl'=4,'tp'=8] {'tp'}, dimensions={1}, use_global_device_ids=true | all-gather | bytes 221184 | tf_op jit(solution)/shard_map/all_gather | solution.py:193
  477.1 0.0 all-to-all-done.4
  477.2 0.5 convolution_bitcast_fusion
  477.6 0.5 fusion.1
  478.1 0.0 copy-done.1
  478.1 0.9 fusion.2
  (14 shorter events, 0.2 us)
Async XLA Ops:
  8.0 1.0 copy-start
  8.1 274.8 %all-gather.4.cloned.1.call-start = ((), (), s32[]{:S(2)}) async-start(), calls=%async_computation.6 | async-start | bytes 7077888 | tf_op jit(solution)/shard_map/all_gather | solution.py:119
  107.6 10.5 %copy-start.5 = (s32[192,8]{0,1:T(8,128)S(1)}, s32[192,8]{0,1:T(8,128)}, u32[]{:S(2)}) copy-start(s32[192,8]{0,1:T(8,128)} %param.11) | copy-start | bytes 18436
  107.6 11.1 %copy-start.4 = (bf16[192,256]{1,0:T(8,128)(2,1)S(1)}, bf16[192,256]{1,0:T(8,128)(2,1)}, u32[]{:S(2)}) copy-start(bf16[192,256]{1,0:T(8,128)(2,1)} %param.10) | copy-start | bytes 294916
  118.4 22.5 %copy-start.8 = (f32[16,256]{1,0:T(8,128)S(1)}, f32[16,256]{1,0:T(8,128)}, u32[]{:S(2)}) copy-start(f32[16,256]{1,0:T(8,128)} %param.19) | copy-start | bytes 49156
  118.7 22.2 %copy-start.6 = (f32[16,256]{1,0:T(8,128)S(1)}, f32[16,256]{1,0:T(8,128)}, u32[]{:S(2)}) copy-start(f32[16,256]{1,0:T(8,128)} %param.17) | copy-start | bytes 49156
  118.7 22.2 %copy-start.7 = (f32[16,256]{1,0:T(8,128)S(1)}, f32[16,256]{1,0:T(8,128)}, u32[]{:S(2)}) copy-start(f32[16,256]{1,0:T(8,128)} %param.18) | copy-start | bytes 49156
  118.7 22.2 %copy-start.10 = (f32[256]{0:T(256)S(1)}, f32[256]{0:T(256)}, u32[]{:S(2)}) copy-start(f32[256]{0:T(256)} %param.13) | copy-start | bytes 3076
  135.8 127.7 %all-to-all-start = ((bf16[32,56,256]{2,1,0:T(8,128)(2,1)}), bf16[32,56,256]{2,1,0:T(8,128)(2,1)S(1)}, u32[]{:S(2)}, u32[]{:S(2)}) async-start(bf16[32,56,256]{2,1,0:T(8,128)(2,1)} %bitcast.3), calls=%async_computation | async-start | bytes 1835008 | tf_op jit(solution)/shard_map/all_to_all | solution.py:160
  309.6 167.5 %all-to-all-start.4 = ((bf16[32,56,256]{2,1,0:T(8,128)(2,1)}), bf16[32,56,256]{2,1,0:T(8,128)(2,1)S(1)}, u32[]{:S(2)}, u32[]{:S(2)}) async-start(bf16[32,56,256]{2,1,0:T(8,128)(2,1)} %bitcast.8), calls=%async_computation.4 | async-start | bytes 1835008 | tf_op jit(solution)/shard_map/all_to_all | solution.py:169
  318.6 97.2 %all-gather.6.cloned.1.call-start = ((), (), s32[]{:S(2)}) async-start(), calls=%async_computation.7 | async-start | bytes 1310720 | tf_op jit(solution)/shard_map/all_gather | solution.py:162
  319.2 143.1 %reduce-scatter.2.cloned.1.call-start = ((), (), s32[]{:S(2)}) async-start(), calls=%async_computation.8 | async-start | bytes 442368 | tf_op jit(solution)/shard_map/reduce_scatter | solution.py:184
  417.2 1.4 copy-start.2
  417.2 1.4 copy-start.3
  417.2 60.9 %copy-start.1 = (bf16[512,256]{1,0:T(8,128)(2,1)}, bf16[512,256]{1,0:T(8,128)(2,1)S(1)}, u32[]{:S(2)}) copy-start(bf16[512,256]{1,0:T(8,128)(2,1)S(1)} %get-tuple-element.11) | copy-start | bytes 786436
  417.2 1.3 copy-start.9
Sparse Core Ops, SparseCore 0:
  118.2 44.0 all-gather.3
  418.6 43.6 reduce-scatter.1
Sparse Core Ops, SparseCore 1:
  321.8 94.0 all-gather.5

commit v7 on v6

--- a/solution.py
+++ b/solution.py
@@ -76,6 +76,16 @@
 
 
 fs = ("fa", "fb", "fc", "fl")
+
+
+def paired(block, axis):
+    if lax.axis_size(axis) == 1:
+        return block
+    other = lax.ppermute(block, axis, [(0, 1), (1, 0)])
+    first = lax.axis_index(axis) == 0
+    return jnp.concatenate(
+        [jnp.where(first, block, other), jnp.where(first, other, block)], axis=0
+    )
 
 
 def layer(
@@ -127,10 +137,9 @@
         ],
         axis=1,
     )
-    block = lax.all_gather(block, "fa", axis=0, tiled=True)
-    block, served = lax.optimization_barrier((block, served))
-    block = lax.all_gather(block, "fb", axis=0, tiled=True)
-    block = lax.all_gather(block, "fc", axis=0, tiled=True)
+    block = paired(block, "fa")
+    block = paired(block, "fb")
+    block = paired(block, "fc")
     block = jnp.pad(block, ((0, 0), (0, width)))
 
     values = tokens.astype(jnp.float32)
@@ -158,7 +167,7 @@
     outgoing = jnp.dot(placing, normed, preferred_element_type=jnp.float32)
     outgoing = outgoing.astype(jnp.bfloat16).reshape(experts, capacity, width)
     incoming = lax.all_to_all(outgoing, fs, split_axis=0, concat_axis=0, tiled=True)
-    incoming, block = lax.optimization_barrier((incoming, block))
+    _, block = lax.optimization_barrier((incoming, block))
     block = lax.all_gather(block, "fl", axis=0, tiled=True)
     chunk = places * capacity // parts
     gathered = lax.all_to_all(

time: 487 us -> 519 us (1.066)
  waiting for transfers between devices: 139 us -> 176 us
  blocking collectives: 296 us -> 276 us
  starting transfers between devices: 14.3 us -> 29.9 us
    all_gather x3 -> x0, blocking collectives: 122 us -> none  [the longest x1 96.5 us: layer(): block = lax.all_gather(block, 'fa', axis=0, tiled=True)]
    all_to_all x0 -> x1, blocking collectives: none -> 101 us  [layer(): lax.all_to_all(outgoing, fs, split_axis=0, concat_axis=0, tiled=True)]
    ppermute x0 -> x3, waiting for transfers between devices: none -> 97.8 us  [paired(): other = lax.ppermute(block, axis, [(0, 1), (1, 0)])]
    all_gather x1, waiting for transfers between devices: 96.5 us -> 33.2 us  [layer(): block = lax.all_gather(block, 'fl', axis=0, tiled=True)]
    ppermute x0 -> x3, starting transfers between devices: none -> 24.9 us  [paired(): other = lax.ppermute(block, axis, [(0, 1), (1, 0)])]
  transfers between devices with their start and end apart: 5 -> 7, of which waited for: 2 -> 5; matrix products, arithmetic and copies ran while one was open for 2% -> 1% of each run, Pallas kernels for 0% -> 0%
where the time goes in v7:
time: 519 us; the launch traced here: 518 us
  blocking collectives  276 us (53%)
  waiting for transfers between devices  176 us (34%)
  starting transfers between devices  29.9 us (6%)
  between operations  15.9 us (3%)
  Pallas kernels  7.97 us (2%)
  local copies, waits for them, and re-layouts  7.36 us (1%)
    all_to_all x1, blocking collectives, layer(): lax.all_to_all(outgoing, fs, split_axis=0, concat_axis=0, tiled=True)  101 us
    ppermute x3, waiting for transfers between devices, paired(): other = lax.ppermute(block, axis, [(0, 1), (1, 0)])  97.8 us
    all_to_all x1, blocking collectives, layer(): lax.all_to_all(jnp.concatenate(pieces, axis=1), fs, split_axis=0, concat_...  97.4 us
    reduce_scatter x1, waiting for transfers between devices, layer(): lax.psum_scatter(partial.reshape(tok_rows, parts, 2 * share_units).transp...  44.8 us
    all_gather x1, waiting for transfers between devices, layer(): block = lax.all_gather(block, 'fl', axis=0, tiled=True)  33.2 us
    ppermute x3, starting transfers between devices, paired(): other = lax.ppermute(block, axis, [(0, 1), (1, 0)])  24.9 us
    all_to_all x1, blocking collectives, layer(): lax.all_to_all(incoming.reshape(parts, chunk, width), 'tp', split_axis=0,...  19.5 us
    all_to_all x1, blocking collectives, layer(): lax.all_to_all(produced, 'tp', split_axis=0, concat_axis=0, tiled=True)  19 us
  transfers between devices with their start and end apart: 7, of which 5 were waited for; matrix products, arithmetic and copies ran while one was open for 1% of the time, Pallas kernels for 0%

profile of v7, /device:TPU:33, one launch (start us, length us, event | category | flops | bytes accessed | tf_op | source)
XLA Modules:
  0.0 518.2 jit_solution(3965760618049972283)
XLA Ops:
  8.0 0.0 copy-start
  8.1 0.1 all-gather.4.cloned.1.call-start
  8.1 1.0 copy-done
  9.1 1.1 multiply_convert_fusion.1
  10.2 97.4 %all_to_all.25 = bf16[32,24,256]{2,1,0:T(8,128)(2,1)S(1)} all-to-all(bf16[32,24,256]{2,1,0:T(8,128)(2,1)S(1)} %pad_maximum_fusion.1), channel_id=1, replica_groups=mesh['grp'=2,'fa'=2,'fb'=2,'fc'=2,'fl'=4,'tp'=8] {'fa','fb','fc','fl'}, dimensions={0} | all-to-all | bytes 786432 | tf_op jit(solution)/shard_map/all_to_all | solution.py:122
  107.6 0.0 copy-start.5
  107.6 0.0 copy-start.4
  107.6 9.4 %all-gather = bf16[64,24,256]{2,1,0:T(8,128)(2,1)S(1)} all-gather(bf16[32,24,256]{2,1,0:T(8,128)(2,1)S(1)} %all_to_all.25), channel_id=2, replica_groups=mesh['grp'=2,'fa'=2,'fb'=2,'fc'=2,'fl'=4,'tp'=8] {'grp'}, dimensions={0}, use_global_device_ids=true | all-gather | bytes 1179648 | tf_op jit(solution)/shard_map/all_gather | solution.py:126
  117.1 1.0 copy.33
  118.0 0.1 all-gather.4.cloned.1.call-update
  118.1 0.1 eq.54
  118.2 0.0 copy-done.5
  118.2 0.1 fusion.3
  118.4 0.3 bitcast_compare_fusion
  118.7 0.0 copy-done.4
  118.7 0.1 fusion.14
  118.8 15.5 %psum.7 = f32[192]{0:T(256)S(1)} all-reduce(f32[192]{0:T(256)S(1)} %fusion.14), channel_id=1, replica_groups=mesh['grp'=2,'fa'=2,'fb'=2,'fc'=2,'fl'=4,'tp'=8] {'tp'}, use_global_device_ids=true, to_apply=%region_3.4 | all-reduce | flops 192 | bytes 1536 | tf_op jit(solution)/shard_map/psum | solution.py:146
  134.3 0.5 convolution_convert_fusion
  134.8 100.9 %all_to_all.26 = bf16[32,56,256]{2,1,0:T(8,128)(2,1)S(1)} all-to-all(bf16[32,56,256]{2,1,0:T(8,128)(2,1)S(1)} %bitcast.47), channel_id=1, replica_groups=mesh['grp'=2,'fa'=2,'fb'=2,'fc'=2,'fl'=4,'tp'=8] {'fa','fb','fc','fl'}, dimensions={0} | all-to-all | bytes 1835008 | tf_op jit(solution)/shard_map/all_to_all | solution.py:169
  235.7 19.5 %all_to_all.27.x_ref = bf16[8,224,256]{2,1,0:T(8,128)(2,1)} all-to-all(bf16[8,224,256]{2,1,0:T(8,128)(2,1)S(1)} %bitcast.48), channel_id=1, replica_groups=mesh['grp'=2,'fa'=2,'fb'=2,'fc'=2,'fl'=4,'tp'=8] {'tp'}, dimensions={0} | all-to-all | bytes 1835008 | tf_op jit(solution)/shard_map/all_to_all | solution.py:173
  255.2 0.0 all-gather.4.cloned.1.call-done.gate_ref.up_ref.down_ref
  255.3 8.0 %expert_mlp.1 = bf16[8,224,256]{2,1,0:T(8,128)(2,1)} custom-call(bf16[8,224,256]{2,1,0:T(8,128)(2,1)} %all_to_all.27.x_ref, bf16[8,1536,256]{2,1,0:T(8,128)(2,1)} %all-gather.4.cloned.1.call-done.gate_ref.up_ref.down_ref, bf16[8,1536,256]{2,1,0:T(8,128)(2,1)} %all-gather.4.cloned.1.call-done.gate_ref.up_ref.down_ref, ...), custom_call_target="tpu_custom_call" | custom-call | flops 1409286144 | bytes 8126464 | tf_op jit(solution)/shard_map/expert_mlp/pallas_call | solution.py:57
  263.2 0.0 copy-start.10
  263.2 19.0 %all_to_all.28 = bf16[8,224,256]{2,1,0:T(8,128)(2,1)} all-to-all(bf16[8,224,256]{2,1,0:T(8,128)(2,1)} %expert_mlp.1), channel_id=1, replica_groups=mesh['grp'=2,'fa'=2,'fb'=2,'fc'=2,'fl'=4,'tp'=8] {'tp'}, dimensions={0} | all-to-all | bytes 1835008 | tf_op jit(solution)/shard_map/all_to_all | solution.py:177
  282.3 4.8 all-to-all-start.4
  287.1 0.1 all-gather.6.cloned.1.call-start
  287.2 0.0 copy-done.8
  287.2 0.0 copy-done.6
  287.2 0.0 copy-done.7
  287.2 0.0 copy-done.10
  287.3 21.0 %collective-permute-start = (bf16[16,768]{1,0:T(8,128)(2,1)S(1)}, bf16[16,768]{1,0:T(8,128)(2,1)S(1)}, u32[]{:S(2)}, u32[]{:S(2)}) collective-permute-start(bf16[16,768]{1,0:T(8,128)(2,1)S(1)} %pad_maximum_fusion.4), channel_id=1, source_target_pairs={{0,128},{128,0},{1,129},{129,1},{2,130},{130,2},{3,131},{131,3},{4... | collective-permute-start | bytes 73736 | tf_op jit(solution)/shard_map/ppermute | solution.py:84
  308.3 74.0 %collective-permute-done = bf16[16,768]{1,0:T(8,128)(2,1)S(1)} collective-permute-done((bf16[16,768]{1,0:T(8,128)(2,1)S(1)}, bf16[16,768]{1,0:T(8,128)(2,1)S(1)}, u32[]{:S(2)}, u32[]{:S(2)}) %collective-permute-start) | collective-permute-done | bytes 24608 | tf_op jit(solution)/shard_map/ppermute | solution.py:84
  382.3 2.0 collective-permute-start.1
  384.3 12.1 %collective-permute-done.1 = bf16[32,768]{1,0:T(8,128)(2,1)S(1)} collective-permute-done((bf16[32,768]{1,0:T(8,128)(2,1)S(1)}, bf16[32,768]{1,0:T(8,128)(2,1)S(1)}, u32[]{:S(2)}, u32[]{:S(2)}) %collective-permute-start.1) | collective-permute-done | bytes 49184 | tf_op jit(solution)/shard_map/ppermute | solution.py:84
  396.4 2.0 collective-permute-start.2
  398.4 11.7 %collective-permute-done.2 = bf16[64,768]{1,0:T(8,128)(2,1)S(1)} collective-permute-done((bf16[64,768]{1,0:T(8,128)(2,1)S(1)}, bf16[64,768]{1,0:T(8,128)(2,1)S(1)}, u32[]{:S(2)}, u32[]{:S(2)}) %collective-permute-start.2) | collective-permute-done | bytes 98336 | tf_op jit(solution)/shard_map/ppermute | solution.py:84
  410.1 0.7 fusion.12
  410.8 0.1 all-gather.6.cloned.1.call-update
  410.9 0.1 reduce-scatter.2.cloned.1.call-start
  411.0 33.2 %all-gather.6.cloned.1.call-done = bf16[512,1024]{1,0:T(8,128)(2,1)} async-done(((bf16[128,1024]{1,0:T(8,128)(2,1)}), bf16[512,1024]{1,0:T(8,128)(2,1)}) %all-gather.6.cloned.1.call-update) | async-done | bytes 1048592 | tf_op jit(solution)/shard_map/all_gather | solution.py:171
  444.2 1.3 copy.34
  445.5 0.1 fusion.21
  445.6 0.0 copy-start.2
  445.6 0.0 copy-start.3
  445.6 0.0 copy-start.1
  445.6 0.0 copy-start.9
  445.7 0.3 fusion
  446.0 0.8 copy.42
  446.8 0.1 reduce-scatter.2.cloned.1.call-update
  446.9 0.0 copy-done.9
  447.0 0.1 fusion.22
  447.0 0.0 copy-done.2
  447.0 0.0 copy-done.3
  447.0 0.7 copy.37
  447.8 0.7 copy.38
  448.5 0.7 copy.39
  449.2 44.8 %reduce-scatter.2.cloned.1.call-done = bf16[1,192,128]{2,1,0:T(8,128)(2,1)} async-done(((bf16[8,192,128]{2,1,0:T(8,128)(2,1)}), bf16[1,192,128]{2,1,0:T(8,128)(2,1)}) %reduce-scatter.2.cloned.1.call-update) | async-done | bytes 49168 | tf_op jit(solution)/shard_map/reduce_scatter | solution.py:193
  494.0 0.9 copy.36
  495.0 13.9 %all_gather.19 = bf16[192,512]{0,1:T(8,128)(2,1)S(1)} all-gather(bf16[192,64]{0,1:T(8,128)(2,1)S(1)} %fusion.16), channel_id=1, replica_groups=mesh['grp'=2,'fa'=2,'fb'=2,'fc'=2,'fl'=4,'tp'=8] {'tp'}, dimensions={1}, use_global_device_ids=true | all-gather | bytes 221184 | tf_op jit(solution)/shard_map/all_gather | solution.py:202
  508.8 0.0 all-to-all-done.4
  508.8 0.5 convolution_bitcast_fusion
  509.3 0.5 fusion.1
  509.8 0.0 copy-done.1
  509.8 0.9 fusion.2
  (21 shorter events, 0.3 us)
Async XLA Ops:
  8.0 1.0 copy-start
  8.1 247.2 %all-gather.4.cloned.1.call-start = ((), (), s32[]{:S(2)}) async-start(), calls=%async_computation.6 | async-start | bytes 7077888 | tf_op jit(solution)/shard_map/all_gather | solution.py:129
  107.6 10.6 %copy-start.5 = (s32[192,8]{0,1:T(8,128)S(1)}, s32[192,8]{0,1:T(8,128)}, u32[]{:S(2)}) copy-start(s32[192,8]{0,1:T(8,128)} %param.11) | copy-start | bytes 18436
  107.6 11.1 %copy-start.4 = (bf16[192,256]{1,0:T(8,128)(2,1)S(1)}, bf16[192,256]{1,0:T(8,128)(2,1)}, u32[]{:S(2)}) copy-start(bf16[192,256]{1,0:T(8,128)(2,1)} %param.10) | copy-start | bytes 294916
  263.2 24.0 %copy-start.8 = (f32[16,256]{1,0:T(8,128)S(1)}, f32[16,256]{1,0:T(8,128)}, u32[]{:S(2)}) copy-start(f32[16,256]{1,0:T(8,128)} %param.19) | copy-start | bytes 49156
  263.2 24.0 %copy-start.6 = (f32[16,256]{1,0:T(8,128)S(1)}, f32[16,256]{1,0:T(8,128)}, u32[]{:S(2)}) copy-start(f32[16,256]{1,0:T(8,128)} %param.17) | copy-start | bytes 49156
  263.2 24.0 %copy-start.7 = (f32[16,256]{1,0:T(8,128)S(1)}, f32[16,256]{1,0:T(8,128)}, u32[]{:S(2)}) copy-start(f32[16,256]{1,0:T(8,128)} %param.18) | copy-start | bytes 49156
  263.2 24.0 %copy-start.10 = (f32[256]{0:T(256)S(1)}, f32[256]{0:T(256)}, u32[]{:S(2)}) copy-start(f32[256]{0:T(256)} %param.13) | copy-start | bytes 3076
  282.3 226.6 %all-to-all-start.4 = ((bf16[32,56,256]{2,1,0:T(8,128)(2,1)}), bf16[32,56,256]{2,1,0:T(8,128)(2,1)S(1)}, u32[]{:S(2)}, u32[]{:S(2)}) async-start(bf16[32,56,256]{2,1,0:T(8,128)(2,1)} %bitcast.8), calls=%async_computation.4 | async-start | bytes 1835008 | tf_op jit(solution)/shard_map/all_to_all | solution.py:178
  287.1 157.1 %all-gather.6.cloned.1.call-start = ((), (), s32[]{:S(2)}) async-start(), calls=%async_computation.7 | async-start | bytes 1310720 | tf_op jit(solution)/shard_map/all_gather | solution.py:171
  287.3 95.0 %collective-permute-start = (bf16[16,768]{1,0:T(8,128)(2,1)S(1)}, bf16[16,768]{1,0:T(8,128)(2,1)S(1)}, u32[]{:S(2)}, u32[]{:S(2)}) collective-permute-start(bf16[16,768]{1,0:T(8,128)(2,1)S(1)} %pad_maximum_fusion.4), channel_id=1, source_target_pairs={{0,128},{128,0},{1,129},{129,1},{2,130},{130,2},{3,131},{131,3},{4... | collective-permute-start | bytes 73736 | tf_op jit(solution)/shard_map/ppermute | solution.py:84
  382.3 14.1 %collective-permute-start.1 = (bf16[32,768]{1,0:T(8,128)(2,1)S(1)}, bf16[32,768]{1,0:T(8,128)(2,1)S(1)}, u32[]{:S(2)}, u32[]{:S(2)}) collective-permute-start(bf16[32,768]{1,0:T(8,128)(2,1)S(1)} %pad_maximum_fusion.3), channel_id=1, source_target_pairs={{0,64},{64,0},{1,65},{65,1},{2,66},{66,2},{3,67},{67,3},{4,68},{68... | collective-permute-start | bytes 147464 | tf_op jit(solution)/shard_map/ppermute | solution.py:84
  396.4 13.6 %collective-permute-start.2 = (bf16[64,768]{1,0:T(8,128)(2,1)S(1)}, bf16[64,768]{1,0:T(8,128)(2,1)S(1)}, u32[]{:S(2)}, u32[]{:S(2)}) collective-permute-start(bf16[64,768]{1,0:T(8,128)(2,1)S(1)} %pad_maximum_fusion.2), channel_id=1, source_target_pairs={{0,32},{32,0},{1,33},{33,1},{2,34},{34,2},{3,35},{35,3},{4,36},{36... | collective-permute-start | bytes 294920 | tf_op jit(solution)/shard_map/ppermute | solution.py:84
  410.9 83.1 %reduce-scatter.2.cloned.1.call-start = ((), (), s32[]{:S(2)}) async-start(), calls=%async_computation.8 | async-start | bytes 442368 | tf_op jit(solution)/shard_map/reduce_scatter | solution.py:193
  445.6 1.5 copy-start.2
  445.6 1.4 copy-start.3
  445.6 64.2 %copy-start.1 = (bf16[512,256]{1,0:T(8,128)(2,1)}, bf16[512,256]{1,0:T(8,128)(2,1)S(1)}, u32[]{:S(2)}) copy-start(bf16[512,256]{1,0:T(8,128)(2,1)S(1)} %get-tuple-element.9) | copy-start | bytes 786436
  445.6 1.3 copy-start.9
Sparse Core Ops, SparseCore 0:
  118.2 44.0 all-gather.3
  447.0 46.9 reduce-scatter.1
Sparse Core Ops, SparseCore 1:
  411.0 33.2 all-gather.5
